TPU v7x, 32 devices: a whole 2x2x4 slice. The times are simulated.
32 devices in a mesh: sp: 8 (over z, x), tp: 4 (over y, core).
Axes of the slice: x: 2, y: 2, z: 4, core: 2. Of those that a mesh axis runs over, the one named last changes fastest.
Arguments:
- mixer_out: bfloat16 [1024, 2048], P('sp', 'tp'), may hold values from -12 to 12
- layer_grad: bfloat16 [1024, 2048], P('sp', 'tp'), may hold values from -6 to 6
- row_scale: float32 [1024], P('sp'), may hold values from 0.3 to 3
- norm_gain: bfloat16 [2048], replicated, may hold values from 0.099609375 to 1.8984375
- routes: int32 [1024, 2], P('sp'), may hold values from 0 to 7, all different within a row; in each aligned block of 128 rows (0 to 127, 128 to 255, ...) at most 64 rows name the same one
- route_weight: float32 [1024, 2], P('sp'), may hold values from 0.05 to 0.35
- expert_gate: bfloat16 [8, 3584, 2048], P('sp', 'tp'), may hold values from -0.125 to 0.125
- expert_up: bfloat16 [8, 3584, 2048], P('sp', 'tp'), may hold values from -0.125 to 0.125
- expert_down: bfloat16 [8, 3584, 2048], P('sp', 'tp'), may hold values from -0.09375 to 0.09375
- query_rows: bfloat16 [1024, 1024], P('sp', 'tp'), may hold values from -6 to 6
- key_rows: bfloat16 [1024, 1024], P('sp', 'tp'), may hold values from -6 to 6
- value_rows: bfloat16 [1024, 1024], P('sp', 'tp'), may hold values from -6 to 6
- retained: bfloat16 [1024, 1024], P('sp', 'tp'), may hold values from -6 to 6
- log_decay: float32 [16, 1024], P('tp', 'sp'), may hold values from -0.8 to 0
- entry_state: float32 [8, 16, 64, 64], P('sp', 'tp'), may hold values from -12 to 12
- out_proj: bfloat16 [1024, 2048], P('tp'), may hold values from -0.1875 to 0.1875
Outputs:
- grad_up: bfloat16 [8, 3584, 2048], P('sp', 'tp')
- grad_down: bfloat16 [8, 3584, 2048], P('sp', 'tp')
- grad_proj: float32 [2048, 1024], P('sp', 'tp')
- grad_query: bfloat16 [1024, 1024], P('sp', 'tp')
- grad_key: bfloat16 [1024, 1024], P('sp', 'tp')
- grad_value: bfloat16 [1024, 1024], P('sp', 'tp')
- stream_grad: bfloat16 [1024, 2048], P('sp', 'tp')
Inputs may be any that keep to these rules, and one draw needn't show every extreme that they name: `routes`: each row names 2 different experts. Among the entries of one block of 128 consecutive rows no expert appears more than 64 times, and in every draw some block names some expert exactly 64 times.
All inputs are finite; a program needn't handle non-finite values.
Results may differ from a plain program's by a relative error of at most 0.025.
Values may be sent and summed in bfloat16 or wider, within the bound.
A program may use at most 64 MiB of HBM per device.

v0:
```python
import jax
import jax.numpy as jnp
from jax import lax
from jax.sharding import PartitionSpec as P


def prefix(array, axis, combine, identity):
    devices, position = (lax.axis_size(axis), lax.axis_index(axis))
    everything = jax.tree.map(lambda part: lax.all_gather(part, axis), array)
    start = jax.tree.map(
        lambda part, zero: jnp.broadcast_to(jnp.asarray(zero, part.dtype), part.shape),
        array,
        identity,
    )

    def step(k, before):
        at = devices - 1 - k
        reached = at > position
        new = combine(before, jax.tree.map(lambda part: part[at], everything))
        return jax.tree.map(lambda a, b: jnp.where(reached, a, b), new, before)

    return lax.fori_loop(0, devices, step, start)


def contract_last(first_op, second_op):
    return lax.dot_general(
        first_op, second_op, (((1,), (1,)), ((), ())), preferred_element_type=jnp.float32
    )


def contract_first(first_op, second_op):
    return lax.dot_general(
        first_op, second_op, (((0,), (0,)), ((), ())), preferred_element_type=jnp.float32
    )


def slot_sources(routes, experts, capacity):
    flat_ids = routes.reshape(-1)
    entries = flat_ids.shape[0]
    onehot = (flat_ids[:, None] == jnp.arange(experts, dtype=jnp.int32)[None, :]).astype(jnp.int32)
    rank_in = jnp.sum(onehot * (jnp.cumsum(onehot, axis=0) - 1), axis=1)
    slot_ids = flat_ids * capacity + rank_in
    matches = slot_ids[None, :] == jnp.arange(experts * capacity, dtype=jnp.int32)[:, None]
    sources = jnp.sum(jnp.where(matches, jnp.arange(entries, dtype=jnp.int32)[None, :], 0), axis=1)
    sources = jnp.where(jnp.any(matches, axis=1), sources, entries)
    return (slot_ids, sources)


def pick_rows(row_block, sources):
    padded = jnp.concatenate(
        [row_block, jnp.zeros((1, row_block.shape[1]), row_block.dtype)], axis=0
    )
    return jnp.take(padded, sources, axis=0)


def span_terms(head_queries, head_keys, head_values, head_gradient, decay_head, incoming_state):
    scale = head_queries.shape[-1] ** (-0.5)
    length = decay_head.shape[1]
    cumul = jnp.cumsum(decay_head, axis=1)
    places = jnp.arange(length)
    causal = (places[:, None] >= places[None, :])[None, :, :]
    spread = cumul[:, :, None] - cumul[:, None, :]
    weights = jnp.where(causal, jnp.exp(jnp.where(causal, spread, 0.0)), 0.0)
    scores = (
        scale
        * jnp.einsum("thd,shd->hts", head_queries, head_keys, precision=lax.Precision.HIGHEST)
        * weights
    )
    pressure = (
        scale
        * jnp.einsum("thd,shd->hts", head_gradient, head_values, precision=lax.Precision.HIGHEST)
        * weights
    )
    grad_query = jnp.einsum("hts,shd->thd", pressure, head_keys, precision=lax.Precision.HIGHEST)
    grad_key = jnp.einsum("hts,thd->shd", pressure, head_queries, precision=lax.Precision.HIGHEST)
    grad_value = jnp.einsum("hts,thd->shd", scores, head_gradient, precision=lax.Precision.HIGHEST)
    ascending_decay = jnp.exp(cumul).T
    grad_query = grad_query + scale * ascending_decay[:, :, None] * jnp.einsum(
        "joy,oiy->joi", head_gradient, incoming_state, precision=lax.Precision.HIGHEST
    )
    state_update = jnp.einsum(
        "olb,oli->lbi",
        head_queries * ascending_decay[:, :, None],
        head_gradient,
        precision=lax.Precision.HIGHEST,
    )
    survive = jnp.exp(cumul[:, -1])
    falling = jnp.exp(cumul[:, -1:] - cumul).T
    return (grad_query, grad_key, grad_value, state_update, survive, falling)


def add_carried(grad_key, grad_value, head_keys, head_values, falling, carried_over_state):
    scale = head_keys.shape[-1] ** (-0.5)
    grad_key = grad_key + scale * falling[:, :, None] * jnp.einsum(
        "upy,ruy->rup", carried_over_state, head_values, precision=lax.Precision.HIGHEST
    )
    grad_value = grad_value + scale * falling[:, :, None] * jnp.einsum(
        "rzw,erz->erw", carried_over_state, head_keys, precision=lax.Precision.HIGHEST
    )
    return (grad_key, grad_value)


def combine_spans(earlier, later_run):
    return (later_run[0] * earlier[0], later_run[1] + later_run[0][:, None, None] * earlier[1])


def body(
    mixer_out,
    layer_grad,
    row_scale,
    norm_gain,
    routes,
    route_weight,
    expert_gate,
    expert_up,
    expert_down,
    query_rows,
    key_rows,
    value_rows,
    retained,
    log_decay,
    entry_state,
    out_proj,
):
    experts = lax.axis_size("sp")
    tp_count = lax.axis_size("tp")
    tokens_here, columns = mixer_out.shape
    fanout = routes.shape[1]
    capacity = 2 * fanout * tokens_here // experts
    slot_ids, sources = slot_sources(routes, experts, capacity)
    gain_all = norm_gain.astype(jnp.float32)
    gain_cols = lax.dynamic_slice_in_dim(gain_all, lax.axis_index("tp") * columns, columns)
    scaled = mixer_out.astype(jnp.float32) * row_scale[:, None]
    normed = (scaled * gain_cols[None, :]).astype(jnp.bfloat16)
    weight_col = route_weight.reshape(-1)[:, None]
    weighted = (weight_col * jnp.repeat(layer_grad.astype(jnp.float32), fanout, axis=0)).astype(
        jnp.bfloat16
    )
    send_normed = pick_rows(jnp.repeat(normed, fanout, axis=0), sources).reshape(
        experts, capacity, columns
    )
    send_grad = pick_rows(weighted, sources).reshape(experts, capacity, columns)
    got_normed, got_grad = (
        lax.all_to_all(send_normed, "sp", split_axis=0, concat_axis=0, tiled=True),
        lax.all_to_all(send_grad, "sp", split_axis=0, concat_axis=0, tiled=True),
    )
    gate_weight = expert_gate[0]
    up_weight = expert_up[0]
    down_weight = expert_down[0]
    model_width = gate_weight.shape[1]
    full_normed, full_grad = (
        lax.all_gather(got_normed, "tp", axis=2, tiled=True),
        lax.all_gather(got_grad, "tp", axis=2, tiled=True),
    )
    normed_rows = full_normed.reshape(-1, model_width)
    grad_rows = full_grad.reshape(-1, model_width)
    gate_pre = contract_last(normed_rows, gate_weight)
    up_pre = contract_last(normed_rows, up_weight)
    act_grad = contract_last(grad_rows, down_weight)
    sigmoid_gate = jax.nn.sigmoid(gate_pre)
    silu_gate = gate_pre * sigmoid_gate
    activation = (silu_gate * up_pre).astype(jnp.bfloat16)
    grad_down = contract_first(activation, grad_rows).astype(jnp.bfloat16)[None]
    up_grad = (act_grad * silu_gate).astype(jnp.bfloat16)
    gate_grad = (act_grad * up_pre * sigmoid_gate * (1.0 + gate_pre * (1.0 - sigmoid_gate))).astype(
        jnp.bfloat16
    )
    grad_up = contract_first(up_grad, normed_rows).astype(jnp.bfloat16)[None]
    partial_value = jnp.dot(gate_grad, gate_weight, preferred_element_type=jnp.float32) + jnp.dot(
        up_grad, up_weight, preferred_element_type=jnp.float32
    )
    shares = lax.psum_scatter(
        partial_value.astype(jnp.bfloat16), "tp", scatter_dimension=1, tiled=True
    )
    returned = lax.all_to_all(
        shares.reshape(experts, capacity, columns), "sp", split_axis=0, concat_axis=0, tiled=True
    )
    per_route = jnp.take(returned.reshape(experts * capacity, columns), slot_ids, axis=0)
    hidden_grad = jnp.sum(
        per_route.reshape(tokens_here, fanout, columns).astype(jnp.float32), axis=1
    ).astype(jnp.bfloat16)
    attend = gain_cols[None, :] * hidden_grad.astype(jnp.float32)
    total_dot = lax.psum(jnp.sum(scaled * attend, axis=1), "tp")
    mean_dot = total_dot[:, None] / (columns * tp_count)
    stream_grad = (
        layer_grad.astype(jnp.float32) + row_scale[:, None] * (attend - scaled * mean_dot)
    ).astype(jnp.bfloat16)
    stream_full = lax.all_gather(stream_grad, "tp", axis=1, tiled=True)
    out_grad = contract_last(stream_full, out_proj).astype(jnp.bfloat16)
    head_count = entry_state.shape[1]
    head_dim = entry_state.shape[-1]

    def split_heads(block):
        return block.astype(jnp.float32).reshape(tokens_here, head_count, head_dim)

    head_keys = split_heads(key_rows)
    head_values = split_heads(value_rows)
    grad_query, grad_key, grad_value, state_update, survive, falling = span_terms(
        split_heads(query_rows),
        head_keys,
        head_values,
        split_heads(out_grad),
        log_decay,
        entry_state[0],
    )
    carried_over_state = prefix(
        (survive, state_update),
        "sp",
        combine_spans,
        (jnp.ones_like(survive), jnp.zeros_like(state_update)),
    )[1]
    grad_key, grad_value = add_carried(
        grad_key, grad_value, head_keys, head_values, falling, carried_over_state
    )
    grad_proj = lax.psum_scatter(
        contract_first(stream_full, retained).astype(jnp.bfloat16),
        "sp",
        scatter_dimension=0,
        tiled=True,
    ).astype(jnp.float32)
    ret_cols = head_count * head_dim
    return (
        grad_up,
        grad_down,
        grad_proj,
        grad_query.reshape(tokens_here, ret_cols).astype(jnp.bfloat16),
        grad_key.reshape(tokens_here, ret_cols).astype(jnp.bfloat16),
        grad_value.reshape(tokens_here, ret_cols).astype(jnp.bfloat16),
        stream_grad,
    )


def solution(mesh):
    in_specs = (
        P("sp", "tp"),
        P("sp", "tp"),
        P("sp"),
        P(),
        P("sp", None),
        P("sp", None),
        P("sp", "tp", None),
        P("sp", "tp", None),
        P("sp", "tp", None),
        P("sp", "tp"),
        P("sp", "tp"),
        P("sp", "tp"),
        P("sp", "tp"),
        P("tp", "sp"),
        P("sp", "tp", None, None),
        P("tp", None),
    )
    out_specs = (
        P("sp", "tp", None),
        P("sp", "tp", None),
        P("sp", "tp"),
        P("sp", "tp"),
        P("sp", "tp"),
        P("sp", "tp"),
        P("sp", "tp"),
    )
    return jax.shard_map(body, mesh=mesh, in_specs=in_specs, out_specs=out_specs, check_vma=False)
```

profile of v0, /device:TPU:11, one launch (start us, length us, event | category | flops | bytes accessed | tf_op | source)
XLA Modules:
  0.0 268.7 jit_solution(12463252049788378154)
XLA Ops:
  7.2 0.9 copy.74
  8.2 0.1 reshape.173
  8.4 0.6 reduce-window.6
  9.0 0.2 slice_reduce_fusion
  9.3 0.2 select_reduce_fusion
  9.5 0.2 fusion.26
  9.7 0.8 dynamic-slice_convert_fusion
  10.5 1.0 multiply_convert_fusion.6
  11.5 0.1 broadcast_in_dim.90
  11.7 1.0 broadcast_in_dim.86
  12.8 0.4 reshape.172
  13.3 0.1 mul.190
  13.6 2.0 gather_fusion.2
  15.5 2.0 gather_fusion.1
  17.5 0.2 broadcast_select_fusion
  17.7 17.0 %all_to_all.15 = bf16[8,64,512]{2,1,0:T(8,128)(2,1)} all-to-all(bf16[8,64,512]{2,1,0:T(8,128)(2,1)S(1)} %bitcast.123), channel_id=1, replica_groups=mesh['sp'=8,'tp'=4] {'sp'}, dimensions={0} | all-to-all | bytes 1048576 | tf_op jit(solution)/shard_map/all_to_all | solution.py:144
  34.8 17.4 %all_to_all.16 = bf16[8,64,512]{2,1,0:T(8,128)(2,1)} all-to-all(bf16[8,64,512]{2,1,0:T(8,128)(2,1)S(1)} %bitcast.122), channel_id=1, replica_groups=mesh['sp'=8,'tp'=4] {'sp'}, dimensions={0} | all-to-all | bytes 1048576 | tf_op jit(solution)/shard_map/all_to_all | solution.py:145
  52.2 0.2 reduce-scatter.3.cloned.1.call-start
  52.4 7.6 %all-gather.7.cloned.1.call-done = bf16[8,64,2048]{2,1,0:T(8,128)(2,1)} async-done(((bf16[8,64,512]{2,1,0:T(8,128)(2,1)}), bf16[8,64,2048]{2,1,0:T(8,128)(2,1)}) %all-gather.7.cloned.1.call-update) | async-done | bytes 2097168 | tf_op jit(solution)/shard_map/all_gather | solution.py:152
  60.0 6.4 %fusion.7 = f32[512,896]{1,0:T(8,128)} fusion(bf16[512,2048]{1,0:T(8,128)(2,1)} %bitcast.142, bf16[1,896,2048]{2,1,0:T(8,128)(2,1)} %param.26), kind=kOutput, calls=%fused_computation.13 | convolution fusion | flops 1879048192 | bytes 7602176 | tf_op jit(solution)/shard_map/dot_general | solution.py:26
  66.5 3.6 %fusion.3 = f32[512,896]{1,0:T(8,128)} fusion(bf16[512,2048]{1,0:T(8,128)(2,1)S(1)} %bitcast.144, bf16[1,896,2048]{2,1,0:T(8,128)(2,1)S(1)} %copy-done.13), kind=kOutput, calls=%fused_computation.9 | convolution fusion | flops 1879048192 | bytes 7602176 | tf_op jit(solution)/shard_map/dot_general | solution.py:26
  70.1 14.1 %all-gather.5.cloned.1.call-done = bf16[8,64,2048]{2,1,0:T(8,128)(2,1)} async-done(((bf16[8,64,512]{2,1,0:T(8,128)(2,1)}), bf16[8,64,2048]{2,1,0:T(8,128)(2,1)}) %all-gather.5.cloned.1.call-update) | async-done | bytes 2097168 | tf_op jit(solution)/shard_map/all_gather | solution.py:153
  84.2 5.8 %multiply_convert_fusion.2 = (bf16[512,896]{1,0:T(8,128)(2,1)S(1)}, f32[512,896]{1,0:T(8,128)S(1)}) fusion(f32[512,896]{1,0:T(8,128)} %fusion.7, bf16[512,2048]{1,0:T(8,128)(2,1)} %bitcast.145, bf16[1,896,2048]{2,1,0:T(8,128)(2,1)} %param.28), kind=kOutput, calls=%fused_computation.22 | convolution fusion | flops 1881800704 | bytes 10354688 | tf_op jit(solution)/shard_map/dot_general | solution.py:26
  90.0 2.3 fusion.1
  92.3 0.5 copy-done.19
  92.9 0.5 copy-done.21
  93.4 4.1 %add_convert_fusion = bf16[512,2048]{1,0:T(8,128)(2,1)} fusion(f32[512,2048]{1,0:T(8,128)S(1)} %fusion.1, bf16[1,896,2048]{2,1,0:T(8,128)(2,1)S(1)} %copy-done.15, f32[512,896]{1,0:T(8,128)S(1)} %copy-done.19, f32[512,896]{1,0:T(8,128)S(1)} %get-tuple-element.213, f32[512,896]{1,0:T(8,128)S(1)} %copy-done.21), kind=kOutput, calls=%fused_computation.6 | convolution fusion | flops 1885732864 | bytes 15466496 | tf_op jit(solution)/shard_map/dot_general | solution.py:169
  97.8 0.5 copy-done.9
  98.4 0.1 mul.210
  98.6 0.1 copy.78
  98.9 0.3 reduce_window_sum.25
  99.2 0.6 dynamic-slice
  100.4 0.2 slice_reduce_fusion.1
  100.6 0.2 dynamic-update-slice
  100.9 11.6 %all-reduce.2 = f32[32]{0:T(128)S(1)} all-reduce(f32[32]{0:T(128)S(1)} %dynamic-update-slice), channel_id=3, replica_groups=mesh['sp'=8,'tp'=4] {'sp'}, use_global_device_ids=true, to_apply=%add.2 | all-reduce | flops 32 | bytes 256
  112.9 0.2 fusion.14
  113.1 15.3 %reduce-scatter.3.cloned.1.call-done = bf16[512,512]{1,0:T(8,128)(2,1)} async-done(((bf16[512,2048]{1,0:T(8,128)(2,1)}), bf16[512,512]{1,0:T(8,128)(2,1)}) %reduce-scatter.3.cloned.1.call-update) | async-done | bytes 524304 | tf_op jit(solution)/shard_map/reduce_scatter | solution.py:172
  128.4 5.5 %all-to-all-start.2 = ((bf16[8,64,512]{2,1,0:T(8,128)(2,1)}), bf16[8,64,512]{2,1,0:T(8,128)(2,1)S(1)}, u32[]{:S(2)}, u32[]{:S(2)}) async-start(bf16[8,64,512]{2,1,0:T(8,128)(2,1)} %bitcast.134), calls=%async_computation.3 | async-start | bytes 1048576 | tf_op jit(solution)/shard_map/all_to_all | solution.py:175
  133.9 6.0 %convert_bitcast_fusion.1 = bf16[1,896,2048]{2,1,0:T(8,128)(2,1)} fusion(bf16[512,896]{1,0:T(8,128)(2,1)} %copy-done.23, bf16[512,2048]{1,0:T(8,128)(2,1)} %bitcast.143), kind=kOutput, calls=%fused_computation.18 | convolution fusion | flops 1880883200 | bytes 6684672 | tf_op jit(solution)/shard_map/dot_general | solution.py:32
  139.9 4.0 %convert_bitcast_fusion = bf16[1,896,2048]{2,1,0:T(8,128)(2,1)} fusion(bf16[512,2048]{1,0:T(8,128)(2,1)S(1)} %bitcast.146, f32[512,896]{1,0:T(8,128)S(1)} %copy-done.22, f32[512,896]{1,0:T(8,128)S(1)} %copy-done.20), kind=kOutput, calls=%fused_computation.17 | convolution fusion | flops 1883635712 | bytes 9437184 | tf_op jit(solution)/shard_map/dot_general | solution.py:32
  143.9 1.9 all-to-all-done.2
  145.8 1.2 gather_fusion
  147.0 0.6 fusion.28
  147.7 0.2 multiply_reduce_fusion
  147.9 5.6 %psum.7 = f32[128]{0:T(128)S(1)} all-reduce(f32[128]{0:T(128)S(1)} %multiply_reduce_fusion), channel_id=1, replica_groups=mesh['sp'=8,'tp'=4] {'tp'}, use_global_device_ids=true, to_apply=%region_8.10 | all-reduce | flops 128 | bytes 1024 | tf_op jit(solution)/shard_map/psum | solution.py:183
  153.5 0.2 add_convert_fusion.1
  153.7 7.9 %all_gather.21 = bf16[128,2048]{1,0:T(8,128)(2,1)S(1)} all-gather(bf16[128,512]{1,0:T(8,128)(2,1)S(1)} %add_convert_fusion.1), channel_id=1, replica_groups=mesh['sp'=8,'tp'=4] {'tp'}, dimensions={1}, use_global_device_ids=true | all-gather | bytes 655360 | tf_op jit(solution)/shard_map/all_gather | solution.py:188
  161.6 0.5 convolution_convert_fusion.1
  162.2 0.2 fusion.30
  162.4 27.2 %all-gather = f32[32,64,64]{2,1,0:T(8,128)S(1)} all-gather(f32[4,64,64]{2,1,0:T(8,128)S(1)} %fusion.30), channel_id=2, replica_groups=mesh['sp'=8,'tp'=4] {'sp'}, dimensions={0}, use_global_device_ids=true | all-gather | bytes 589824 | tf_op jit(solution)/shard_map/all_gather | solution.py:9
  189.6 1.5 convolution_convert_fusion
  191.1 1.1 while.16
  192.2 0.3 fusion.16
  192.5 0.2 fusion.22
  192.7 0.7 copy.87
  193.5 0.2 fusion.17
  193.7 0.2 fusion.15
  193.9 0.2 fusion.23
  194.2 0.7 copy.86
  194.9 0.2 fusion.18
  195.1 0.4 fusion.24
  195.5 0.7 copy.85
  196.3 64.3 %reduce-scatter.5.cloned.1.call-done = bf16[256,256]{1,0:T(8,128)(2,1)} async-done(((bf16[2048,256]{1,0:T(8,128)(2,1)}), bf16[256,256]{1,0:T(8,128)(2,1)}) %reduce-scatter.5.cloned.1.call-update) | async-done | bytes 131088 | tf_op jit(solution)/shard_map/reduce_scatter | solution.py:215
  260.5 1.6 convert_element_type.93
  (100 shorter events, 2.8 us)
Async XLA Ops:
  7.2 154.4 %copy-start = (bf16[256,2048]{1,0:T(8,128)(2,1)S(1)}, bf16[256,2048]{1,0:T(8,128)(2,1)}, u32[]{:S(2)}) copy-start(bf16[256,2048]{1,0:T(8,128)(2,1)} %param.35) | copy-start | bytes 3145732
  7.2 6.0 %copy-start.12 = (f32[128,2]{0,1:T(2,128)S(1)}, f32[128,2]{0,1:T(2,128)}, u32[]{:S(2)}) copy-start(f32[128,2]{0,1:T(2,128)} %param.25) | copy-start | bytes 3076
  7.2 52.8 %all-gather.7.cloned.1.call-start = ((), (), s32[]{:S(2)}) async-start(), calls=%async_computation.6 | async-start | bytes 2621440 | tf_op jit(solution)/shard_map/all_gather | solution.py:152
  34.7 49.4 %all-gather.5.cloned.1.call-start = ((), (), s32[]{:S(2)}) async-start(), calls=%async_computation.5 | async-start | bytes 2621440 | tf_op jit(solution)/shard_map/all_gather | solution.py:153
  52.2 76.2 %reduce-scatter.3.cloned.1.call-start = ((), (), s32[]{:S(2)}) async-start(), calls=%async_computation.7 | async-start | bytes 2621440 | tf_op jit(solution)/shard_map/reduce_scatter | solution.py:172
  60.0 6.5 %copy-start.13 = (bf16[1,896,2048]{2,1,0:T(8,128)(2,1)S(1)}, bf16[1,896,2048]{2,1,0:T(8,128)(2,1)}, u32[]{:S(2)}) copy-start(bf16[1,896,2048]{2,1,0:T(8,128)(2,1)} %param.27) | copy-start | bytes 11010052
  60.0 6.5 %copy-start.16 = (bf16[8,64,2048]{2,1,0:T(8,128)(2,1)S(1)}, bf16[8,64,2048]{2,1,0:T(8,128)(2,1)}, u32[]{:S(2)}) copy-start(bf16[8,64,2048]{2,1,0:T(8,128)(2,1)} %all-gather.7.cloned.1.call-done) | copy-start | bytes 6291460
  84.1 5.8 %copy-start.14 = (bf16[1,896,2048]{2,1,0:T(8,128)(2,1)S(1)}, bf16[1,896,2048]{2,1,0:T(8,128)(2,1)}, u32[]{:S(2)}) copy-start(bf16[1,896,2048]{2,1,0:T(8,128)(2,1)} %param.27) | copy-start | bytes 11010052
  89.9 2.4 copy-start.23
  90.0 2.4 copy-start.15
  90.0 2.9 %copy-start.19 = (f32[512,896]{1,0:T(8,128)S(1)}, f32[512,896]{1,0:T(8,128)}, u32[]{:S(2)}) copy-start(f32[512,896]{1,0:T(8,128)} %fusion.7) | copy-start | bytes 5505028
  90.0 3.5 %copy-start.21 = (f32[512,896]{1,0:T(8,128)S(1)}, f32[512,896]{1,0:T(8,128)}, u32[]{:S(2)}) copy-start(f32[512,896]{1,0:T(8,128)} %fusion.3) | copy-start | bytes 5505028
  97.6 0.7 copy-start.9
  97.6 1.2 copy-start.6
  97.6 1.3 copy-start.11
  97.6 1.6 copy-start.18
  97.6 14.9 %copy-start.7 = (bf16[128,256]{1,0:T(8,128)(2,1)S(1)}, bf16[128,256]{1,0:T(8,128)(2,1)}, u32[]{:S(2)}) copy-start(bf16[128,256]{1,0:T(8,128)(2,1)} %param.30) | copy-start | bytes 196612
  97.6 15.0 %copy-start.8 = (bf16[128,256]{1,0:T(8,128)(2,1)S(1)}, bf16[128,256]{1,0:T(8,128)(2,1)}, u32[]{:S(2)}) copy-start(bf16[128,256]{1,0:T(8,128)(2,1)} %param.31) | copy-start | bytes 196612
  128.4 17.4 %all-to-all-start.2 = ((bf16[8,64,512]{2,1,0:T(8,128)(2,1)}), bf16[8,64,512]{2,1,0:T(8,128)(2,1)S(1)}, u32[]{:S(2)}, u32[]{:S(2)}) async-start(bf16[8,64,512]{2,1,0:T(8,128)(2,1)} %bitcast.134), calls=%async_computation.3 | async-start | bytes 1048576 | tf_op jit(solution)/shard_map/all_to_all | solution.py:175
  133.9 126.6 %reduce-scatter.5.cloned.1.call-start = ((), (), s32[]{:S(2)}) async-start(), calls=%async_computation.8 | async-start | bytes 1179648 | tf_op jit(solution)/shard_map/reduce_scatter | solution.py:215
  133.9 6.0 %copy-start.17 = (bf16[8,64,2048]{2,1,0:T(8,128)(2,1)S(1)}, bf16[8,64,2048]{2,1,0:T(8,128)(2,1)}, u32[]{:S(2)}) copy-start(bf16[8,64,2048]{2,1,0:T(8,128)(2,1)} %all-gather.5.cloned.1.call-done) | copy-start | bytes 6291460
  133.9 6.0 %copy-start.20 = (f32[512,896]{1,0:T(8,128)S(1)}, f32[512,896]{1,0:T(8,128)}, u32[]{:S(2)}) copy-start(f32[512,896]{1,0:T(8,128)} %fusion.7) | copy-start | bytes 5505028
  133.9 6.0 %copy-start.22 = (f32[512,896]{1,0:T(8,128)S(1)}, f32[512,896]{1,0:T(8,128)}, u32[]{:S(2)}) copy-start(f32[512,896]{1,0:T(8,128)} %fusion.3) | copy-start | bytes 5505028
  143.9 3.8 %copy-start.1 = (bf16[128,512]{1,0:T(8,128)(2,1)S(1)}, bf16[128,512]{1,0:T(8,128)(2,1)}, u32[]{:S(2)}) copy-start(bf16[128,512]{1,0:T(8,128)(2,1)} %param.20) | copy-start | bytes 393220
  143.9 3.8 %copy-start.10 = (f32[128]{0:T(128)S(1)}, f32[128]{0:T(128)}, u32[]{:S(2)}) copy-start(f32[128]{0:T(128)} %param.22) | copy-start | bytes 1540
  143.9 9.6 %copy-start.2 = (bf16[128,512]{1,0:T(8,128)(2,1)S(1)}, bf16[128,512]{1,0:T(8,128)(2,1)}, u32[]{:S(2)}) copy-start(bf16[128,512]{1,0:T(8,128)(2,1)} %param.21) | copy-start | bytes 393220
  153.5 36.1 %copy-start.5 = (bf16[128,256]{1,0:T(8,128)(2,1)S(1)}, bf16[128,256]{1,0:T(8,128)(2,1)}, u32[]{:S(2)}) copy-start(bf16[128,256]{1,0:T(8,128)(2,1)} %param.32) | copy-start | bytes 196612
  153.6 37.4 %copy-start.3 = (bf16[128,512]{1,0:T(8,128)(2,1)}, bf16[128,512]{1,0:T(8,128)(2,1)S(1)}, u32[]{:S(2)}) copy-start(bf16[128,512]{1,0:T(8,128)(2,1)S(1)} %add_convert_fusion.1) | copy-start | bytes 393220
  191.1 3.9 %copy-start.4 = (f32[1,4,64,64]{3,2,1,0:T(8,128)S(1)}, f32[1,4,64,64]{3,2,1,0:T(8,128)}, u32[]{:S(2)}) copy-start(f32[1,4,64,64]{3,2,1,0:T(8,128)} %param.34) | copy-start | bytes 196612
Sparse Core Ops, SparseCore 0:
  34.8 25.0 all-gather.6
  61.6 22.5 all-gather.4
  97.7 30.6 reduce-scatter.2
  191.2 69.2 reduce-scatter.4
where the time goes:
time: 273 us; the launch traced here: 269 us
  waiting for transfers between devices  103 us (38%)
  blocking collectives  86.6 us (32%)
  matrix products  36.5 us (13%)
  between operations  15 us (5%)
  local copies, waits for them, and re-layouts  14.6 us (5%)
  other arithmetic  6.82 us (2%)
  starting transfers between devices  5.8 us (2%)
    reduce_scatter x1, waiting for transfers between devices, body(): lax.psum_scatter(contract_first(stream_full, retained).astype(jnp.bfloat1...  64.3 us
    all_gather x1, blocking collectives, prefix(): everything = jax.tree.map(lambda part: lax.all_gather(part, axis), array)  27.2 us
    all_to_all x1, blocking collectives, body(): lax.all_to_all(send_grad, 'sp', split_axis=0, concat_axis=0, tiled=True)  17.4 us
    all_to_all x1, blocking collectives, body(): lax.all_to_all(send_normed, 'sp', split_axis=0, concat_axis=0, tiled=True)  17 us
    dot_general x4, matrix products, contract_last(): lax.dot_general(first_op, second_op, (((1,), (1,)), ((), ())), preferred_...  16.3 us
    reduce_scatter x1, waiting for transfers between devices, body(): lax.psum_scatter(partial_value.astype(jnp.bfloat16), 'tp', scatter_dimens...  15.3 us
    all_gather x1, waiting for transfers between devices, body(): lax.all_gather(got_grad, 'tp', axis=2, tiled=True)  14.1 us
    unnamed x1, blocking collectives  11.6 us
  transfers between devices with their start and end apart: 5, of which 5 were waited for; matrix products, arithmetic and copies ran while one was open for 10% of the time, Pallas kernels for 0%

commit v1 on v0

v1 whole, which is shorter than its diff:
```python
import functools

import jax
import jax.numpy as jnp
from jax import lax
from jax.experimental import pallas as pl
from jax.experimental.pallas import tpu as pltpu
from jax.sharding import PartitionSpec as P

MESH = pl.DeviceIdType.MESH
VMEM = pl.BlockSpec(memory_space=pltpu.VMEM)
BF16, F32 = jnp.bfloat16, jnp.float32


def remote(src, dst, send_sem, recv_sem, device):
    return pltpu.make_async_remote_copy(
        src_ref=src, dst_ref=dst, send_sem=send_sem, recv_sem=recv_sem,
        device_id=device, device_id_type=MESH,
    )


def greet(devices):
    barrier = pltpu.get_barrier_semaphore()
    for device in devices:
        pl.semaphore_signal(barrier, inc=1, device_id=device, device_id_type=MESH)
    pl.semaphore_wait(barrier, len(devices))


class Place:
    def __init__(self, n, tp):
        self.n, self.tp, self.rows = n, tp, tp // 2
        self.s, self.t = lax.axis_index("sp"), lax.axis_index("tp")
        self.core, self.y = lax.rem(self.t, 2), self.t // 2
        self.twin_t = self.t + 1 - 2 * self.core
        self.twin = (self.s, self.twin_t)

    def to_sp(self, k):
        return lax.rem(self.s + k, self.n)

    def from_sp(self, k):
        return lax.rem(self.s + self.n - k, self.n)

    def to_y(self, k):
        return 2 * lax.rem(self.y + k, self.rows) + self.core

    def from_y(self, k):
        return 2 * lax.rem(self.y + self.rows - k, self.rows) + self.core

    def sp_peers(self):
        return [(self.to_sp(k), self.t) for k in range(1, self.n)]

    def tp_peers(self):
        return [(self.s, lax.rem(self.t + k, self.tp)) for k in range(1, self.tp)]

    def y_peers(self):
        return [(self.s, self.to_y(k)) for k in range(1, self.rows)] + [self.twin]


def dispatch_kernel(n, tp, normed_ref, grad_ref, full_n_ref, full_g_ref, buf, s1, r1, s2, r2, s3, r3):
    at = Place(n, tp)
    capacity, columns = normed_ref.shape[1:]
    greet(at.sp_peers() + at.y_peers())
    inputs = (normed_ref, grad_ref)
    pending = []

    def start(copy):
        copy.start()
        pending.append(copy)

    def spread(kind, source, block):
        for k in range(1, at.rows):
            start(remote(block, buf.at[kind, at.t, source], s2.at[kind, k - 1, source],
                         r2.at[kind, k - 1, source], (at.s, at.to_y(k))))
        start(remote(block, buf.at[kind, at.t, source], s3.at[kind, 0, source],
                     r3.at[kind, 0, source], at.twin))

    def hand_on(kind, source):
        for k in range(1, at.rows):
            slot = buf.at[kind, at.from_y(k), source]
            remote(slot, slot, s2.at[kind, k - 1, source], r2.at[kind, k - 1, source], at.twin).wait_recv()
            start(remote(slot, slot, s3.at[kind, k, source], r3.at[kind, k, source], at.twin))

    for kind in range(2):
        spread(kind, at.s, inputs[kind].at[at.s])
        for k in range(1, n):
            there = at.to_sp(k)
            start(remote(inputs[kind].at[there], buf.at[kind, at.t, at.s], s1.at[kind, there],
                         r1.at[kind, at.s], (there, at.t)))
        buf[kind, at.t, at.s] = inputs[kind][at.s]
    lag = [(kind, at.s) for kind in range(2)]
    for kind in range(2):
        for k in range(1, n):
            source = at.from_sp(k)
            slot = buf.at[kind, at.t, source]
            remote(slot, slot, s1.at[kind, source], r1.at[kind, source], at.twin).wait_recv()
            spread(kind, source, slot)
            lag.append((kind, source))
            if len(lag) > 3:
                hand_on(*lag.pop(0))
    for item in lag:
        hand_on(*item)
    for kind in range(2):
        for k in range(n):
            source = at.from_sp(k)
            for hop in range(at.rows):
                owner = at.twin_t if hop == 0 else lax.rem(at.from_y(hop) + 1 - 2 * at.core, tp)
                slot = buf.at[kind, owner, source]
                remote(slot, slot, s3.at[kind, hop, source], r3.at[kind, hop, source], at.twin).wait_recv()
    for kind, out in enumerate((full_n_ref, full_g_ref)):
        for t in range(tp):
            out[:, t * columns:(t + 1) * columns] = buf[kind, t].reshape(n * capacity, columns)
    for copy in pending:
        copy.wait_send()


def dispatch(n, tp, send_normed, send_grad):
    _, capacity, columns = send_normed.shape
    rows = tp // 2
    full = jax.ShapeDtypeStruct((n * capacity, tp * columns), BF16)
    dma = pltpu.SemaphoreType.DMA
    return pl.pallas_call(
        functools.partial(dispatch_kernel, n, tp),
        out_shape=(full, full),
        in_specs=[VMEM] * 2,
        out_specs=(VMEM, VMEM),
        scratch_shapes=[
            pltpu.VMEM((2, tp, n, capacity, columns), BF16),
            dma((2, n)), dma((2, n)),
            dma((2, rows, n)), dma((2, rows, n)),
            dma((2, rows, n)), dma((2, rows, n)),
        ],
        compiler_params=pltpu.CompilerParams(collective_id=1, has_side_effects=True),
        name="dispatch",
    )(send_normed, send_grad)


def eye(size):
    return lax.broadcasted_iota(jnp.int32, (size, size), 0) == lax.broadcasted_iota(jnp.int32, (size, size), 1)


def return_kernel(n, tp, part_ref, pick_ref, mixer_ref, layer_ref, scale_ref, gain_ref, kept_ref, surv_ref,
                  stream_ref, full_ref, kept_all_ref, surv_all_ref,
                  b1, s1buf, b2, total, back, stat, sbuf,
                  sa, ra, sb, rb, sc, rc, sd, rd, se, re, sf, rf, sk, rk, sv, rv):
    at = Place(n, tp)
    tokens, columns = mixer_ref.shape
    capacity = back.shape[1]
    pair = at.s + 1 - 2 * lax.rem(at.s, 2)
    greet(at.sp_peers() + at.tp_peers())
    pending = []

    def start(copy):
        copy.start()
        pending.append(copy)

    for k in range(at.rows):
        yy = lax.rem(at.y + k, at.rows)
        cols = pl.ds(pl.multiple_of((2 * yy + 1 - at.core) * columns, 128), columns)
        start(remote(part_ref.at[:, cols], b1.at[yy], sa.at[yy], ra.at[yy], at.twin))
    for k in range(1, n):
        there = at.to_sp(k)
        start(remote(surv_ref, surv_all_ref.at[at.s], sv.at[there], rv.at[at.s], (there, at.t)))
    surv_all_ref[at.s] = surv_ref[...]
    for k in range(2, n, 2):
        there = at.to_sp(k)
        start(remote(kept_ref, kept_all_ref.at[at.s], sk.at[0, there], rk.at[at.s], (there, at.t)))
    start(remote(kept_ref, kept_all_ref.at[at.s], sk.at[1, at.s], rk.at[at.s], (pair, at.t)))
    kept_all_ref[at.s] = kept_ref[...]

    for k in range(at.rows):
        yy = lax.rem(at.y + k, at.rows)
        remote(b1.at[yy], b1.at[yy], sa.at[yy], ra.at[yy], at.twin).wait_recv()
    order = [at.to_sp(k) for k in range(1, n)] + [at.s]

    def rows_of(block):
        return pl.ds(pl.multiple_of(block * capacity, capacity), capacity)

    def mine(block, yy):
        cols = pl.ds(pl.multiple_of((2 * yy + at.core) * columns, 128), columns)
        return part_ref[rows_of(block), cols].astype(F32) + b1[yy, rows_of(block), :].astype(F32)

    for block in order:
        for k in range(1, at.rows):
            yy = lax.rem(at.y + k, at.rows)
            s1buf[k - 1, block] = mine(block, yy).astype(BF16)
            start(remote(s1buf.at[k - 1, block], b2.at[k - 1, block], sb.at[k - 1, block],
                         rb.at[k - 1, block], (at.s, at.to_y(k))))
    for place, block in enumerate(order):
        summed = mine(block, at.y)
        for k in range(1, at.rows):
            slot = b2.at[k - 1, block]
            remote(slot, slot, sb.at[k - 1, block], rb.at[k - 1, block], at.twin).wait_recv()
            summed = summed + b2[k - 1, block].astype(F32)
        if place < n - 1:
            total[block] = summed.astype(BF16)
            start(remote(total.at[block], back.at[at.s], sc.at[block], rc.at[at.s], (block, at.t)))
        else:
            back[at.s] = summed.astype(BF16)
    for k in range(2, n, 2):
        source = at.from_sp(k)
        slot = kept_all_ref.at[source]
        remote(slot, slot, sk.at[0, source], rk.at[source], at.twin).wait_recv()
        start(remote(slot, slot, sk.at[1, source], rk.at[source], (pair, at.t)))
    for k in range(1, n):
        source = at.from_sp(k)
        slot = back.at[source]
        remote(slot, slot, sc.at[source], rc.at[source], at.twin).wait_recv()
    hidden = jnp.dot(pick_ref[...], back[...].reshape(n * capacity, columns), preferred_element_type=F32)
    attend = gain_ref[...] * hidden.astype(BF16).astype(F32)
    row_scale = scale_ref[:, 0:1]
    scaled = mixer_ref[...].astype(F32) * row_scale
    column = jnp.sum(scaled * attend, axis=1, keepdims=True)
    diagonal = eye(tokens)
    row = jnp.sum(jnp.where(diagonal, column, 0.0), axis=0, keepdims=True)
    stat[at.t] = jnp.broadcast_to(row, (8, tokens))
    for k in range(1, tp):
        there = lax.rem(at.t + k, tp)
        start(remote(stat.at[at.t], stat.at[at.t], sd.at[there], rd.at[at.t], (at.s, there)))
    for k in range(1, tp):
        source = lax.rem(at.t + tp - k, tp)
        remote(stat.at[source], stat.at[source], sd.at[source], rd.at[source], at.twin).wait_recv()
    summed_row = jnp.sum(stat[...], axis=0)[0:1, :]
    mean_dot = jnp.sum(jnp.where(diagonal, summed_row, 0.0), axis=1, keepdims=True) / (columns * tp)
    stream = (layer_ref[...].astype(F32) + row_scale * (attend - scaled * mean_dot)).astype(BF16)
    stream_ref[...] = stream
    sbuf[at.t] = stream
    for k in range(1, at.rows):
        start(remote(sbuf.at[at.t], sbuf.at[at.t], se.at[k - 1], re.at[k - 1], (at.s, at.to_y(k))))
    start(remote(sbuf.at[at.t], sbuf.at[at.t], sf.at[0], rf.at[0], at.twin))
    for k in range(1, at.rows):
        slot = sbuf.at[at.from_y(k)]
        remote(slot, slot, se.at[k - 1], re.at[k - 1], at.twin).wait_recv()
        start(remote(slot, slot, sf.at[k], rf.at[k], at.twin))
    for hop in range(at.rows):
        owner = at.twin_t if hop == 0 else lax.rem(at.from_y(hop) + 1 - 2 * at.core, tp)
        slot = sbuf.at[owner]
        remote(slot, slot, sf.at[hop], rf.at[hop], at.twin).wait_recv()
    for t in range(tp):
        full_ref[:, t * columns:(t + 1) * columns] = sbuf[t]
    for k in range(1, n):
        source = at.from_sp(k)
        slot = surv_all_ref.at[source]
        remote(slot, slot, sv.at[source], rv.at[source], at.twin).wait_recv()
    for k in range(0, n, 2):
        source = lax.rem(pair + n - k, n)
        slot = kept_all_ref.at[source]
        remote(slot, slot, sk.at[0, source], rk.at[source], at.twin).wait_recv()
    for copy in pending:
        copy.wait_send()


def give_back(n, tp, part, pick, mixer, layer, row_scale, gain, kept, surv):
    tokens, columns = mixer.shape
    rows, capacity = tp // 2, part.shape[0] // n
    dma = pltpu.SemaphoreType.DMA
    return pl.pallas_call(
        functools.partial(return_kernel, n, tp),
        out_shape=(
            jax.ShapeDtypeStruct((tokens, columns), BF16),
            jax.ShapeDtypeStruct((tokens, tp * columns), BF16),
            jax.ShapeDtypeStruct((n,) + kept.shape, BF16),
            jax.ShapeDtypeStruct((n,) + surv.shape, F32),
        ),
        in_specs=[VMEM] * 8,
        out_specs=(VMEM,) * 4,
        scratch_shapes=[
            pltpu.VMEM((rows, n * capacity, columns), BF16),
            pltpu.VMEM((rows, n, capacity, columns), BF16),
            pltpu.VMEM((rows, n, capacity, columns), BF16),
            pltpu.VMEM((n, capacity, columns), BF16),
            pltpu.VMEM((n, capacity, columns), BF16),
            pltpu.VMEM((tp, 8, tokens), F32),
            pltpu.VMEM((tp, tokens, columns), BF16),
            dma((rows,)), dma((rows,)),
            dma((rows, n)), dma((rows, n)),
            dma((n,)), dma((n,)),
            dma((tp,)), dma((tp,)),
            dma((rows,)), dma((rows,)),
            dma((rows,)), dma((rows,)),
            dma((2, n)), dma((n,)),
            dma((n,)), dma((n,)),
        ],
        compiler_params=pltpu.CompilerParams(collective_id=2, has_side_effects=True),
        name="give_back",
    )(part, pick, mixer, layer, row_scale, gain, kept, surv)


def exchange_kernel(n, tp, state_ref, weight_ref, cut_ref, carried_ref, cols_ref, sbuf, cbuf, su, ru, sc, rc, sd, rd):
    at = Place(n, tp)
    tokens = cut_ref.shape[1]
    half = tokens // 2
    greet(at.sp_peers() + [at.twin])
    pending = []

    def start(copy):
        copy.start()
        pending.append(copy)

    own = pl.ds(pl.multiple_of(at.core * half, half), half)
    other = pl.ds(pl.multiple_of((1 - at.core) * half, half), half)
    for k in range(1, n):
        there = at.to_sp(k)
        start(remote(state_ref, sbuf.at[at.s], su.at[there], ru.at[at.s], (there, at.t)))
        start(remote(cut_ref.at[there, own], cbuf.at[at.s, own], sc.at[there], rc.at[at.s], (there, at.t)))
    sbuf[at.s] = state_ref[...]
    cbuf[at.s] = cut_ref[at.s]
    for k in range(1, n):
        source = at.from_sp(k)
        slot = cbuf.at[source, own]
        remote(slot, slot, sc.at[source], rc.at[source], at.twin).wait_recv()
        start(remote(slot, slot, sd.at[source], rd.at[source], at.twin))
    total = jnp.zeros(carried_ref.shape, F32)
    for k in range(1, n):
        source = at.from_sp(k)
        slot = sbuf.at[source]
        remote(slot, slot, su.at[source], ru.at[source], at.twin).wait_recv()
        total = total + weight_ref[source] * sbuf[source].astype(F32)
    carried_ref[...] = total
    for k in range(1, n):
        source = at.from_sp(k)
        slot = cbuf.at[source, other]
        remote(slot, slot, sd.at[source], rd.at[source], at.twin).wait_recv()
    cols_ref[...] = cbuf[...]
    for copy in pending:
        copy.wait_send()


def exchange(n, tp, state, weight, cut):
    dma = pltpu.SemaphoreType.DMA
    return pl.pallas_call(
        functools.partial(exchange_kernel, n, tp),
        out_shape=(jax.ShapeDtypeStruct(state.shape, F32), jax.ShapeDtypeStruct(cut.shape, BF16)),
        in_specs=[VMEM] * 3,
        out_specs=(VMEM, VMEM),
        scratch_shapes=[
            pltpu.VMEM((n,) + state.shape, BF16),
            pltpu.VMEM(cut.shape, BF16),
            dma((n,)), dma((n,)), dma((n,)), dma((n,)), dma((n,)), dma((n,)),
        ],
        compiler_params=pltpu.CompilerParams(collective_id=3, has_side_effects=True),
        name="exchange",
    )(state, weight, cut)


def contract_last(first_op, second_op):
    return lax.dot_general(
        first_op, second_op, (((1,), (1,)), ((), ())), preferred_element_type=jnp.float32
    )


def contract_first(first_op, second_op):
    return lax.dot_general(
        first_op, second_op, (((0,), (0,)), ((), ())), preferred_element_type=jnp.float32
    )


def span_terms(head_queries, head_keys, head_values, head_gradient, decay_head, incoming_state):
    scale = head_queries.shape[-1] ** (-0.5)
    length = decay_head.shape[1]
    cumul = jnp.cumsum(decay_head, axis=1)
    places = jnp.arange(length)
    causal = (places[:, None] >= places[None, :])[None, :, :]
    spread = cumul[:, :, None] - cumul[:, None, :]
    weights = jnp.where(causal, jnp.exp(jnp.where(causal, spread, 0.0)), 0.0)
    scores = (
        scale
        * jnp.einsum("thd,shd->hts", head_queries, head_keys, precision=lax.Precision.HIGHEST)
        * weights
    )
    pressure = (
        scale
        * jnp.einsum("thd,shd->hts", head_gradient, head_values, precision=lax.Precision.HIGHEST)
        * weights
    )
    grad_query = jnp.einsum("hts,shd->thd", pressure, head_keys, precision=lax.Precision.HIGHEST)
    grad_key = jnp.einsum("hts,thd->shd", pressure, head_queries, precision=lax.Precision.HIGHEST)
    grad_value = jnp.einsum("hts,thd->shd", scores, head_gradient, precision=lax.Precision.HIGHEST)
    ascending_decay = jnp.exp(cumul).T
    grad_query = grad_query + scale * ascending_decay[:, :, None] * jnp.einsum(
        "joy,oiy->joi", head_gradient, incoming_state, precision=lax.Precision.HIGHEST
    )
    state_update = jnp.einsum(
        "olb,oli->lbi",
        head_queries * ascending_decay[:, :, None],
        head_gradient,
        precision=lax.Precision.HIGHEST,
    )
    survive = jnp.exp(cumul[:, -1])
    falling = jnp.exp(cumul[:, -1:] - cumul).T
    return (grad_query, grad_key, grad_value, state_update, survive, falling)


def add_carried(grad_key, grad_value, head_keys, head_values, falling, carried_over_state):
    scale = head_keys.shape[-1] ** (-0.5)
    grad_key = grad_key + scale * falling[:, :, None] * jnp.einsum(
        "upy,ruy->rup", carried_over_state, head_values, precision=lax.Precision.HIGHEST
    )
    grad_value = grad_value + scale * falling[:, :, None] * jnp.einsum(
        "rzw,erz->erw", carried_over_state, head_keys, precision=lax.Precision.HIGHEST
    )
    return (grad_key, grad_value)


def body(
    mixer_out,
    layer_grad,
    row_scale,
    norm_gain,
    routes,
    route_weight,
    expert_gate,
    expert_up,
    expert_down,
    query_rows,
    key_rows,
    value_rows,
    retained,
    log_decay,
    entry_state,
    out_proj,
):
    experts = lax.axis_size("sp")
    tp_count = lax.axis_size("tp")
    tokens_here, columns = mixer_out.shape
    fanout = routes.shape[1]
    capacity = 2 * fanout * tokens_here // experts
    slots = experts * capacity
    chosen = routes[:, :, None] == jnp.arange(experts, dtype=jnp.int32)[None, None, :]
    counts = jnp.sum(chosen, axis=1).astype(BF16)
    places = jnp.arange(tokens_here)
    before = (places[:, None] > places[None, :]).astype(BF16)
    ranks = jnp.dot(before, counts, preferred_element_type=F32).astype(jnp.int32)
    rank_in = jnp.sum(jnp.where(chosen, ranks[:, None, :], 0), axis=2)
    slot_ids = routes * capacity + rank_in
    hits = slot_ids[:, :, None] == jnp.arange(slots, dtype=jnp.int32)[None, None, :]
    pick = jnp.any(hits, axis=1).astype(BF16)
    slot_weight = jnp.sum(jnp.where(hits, route_weight[:, :, None], 0.0), axis=(0, 1))
    gain_all = norm_gain.astype(F32)
    gain_cols = lax.dynamic_slice_in_dim(gain_all, lax.axis_index("tp") * columns, columns)
    scaled = mixer_out.astype(F32) * row_scale[:, None]
    normed = (scaled * gain_cols[None, :]).astype(BF16)
    send_normed = contract_first(pick, normed).astype(BF16).reshape(experts, capacity, columns)
    send_grad = (slot_weight[:, None] * contract_first(pick, layer_grad)).astype(BF16).reshape(
        experts, capacity, columns
    )
    normed_rows, grad_rows = dispatch(experts, tp_count, send_normed, send_grad)
    gate_weight = expert_gate[0]
    up_weight = expert_up[0]
    down_weight = expert_down[0]
    gate_pre = contract_last(normed_rows, gate_weight)
    up_pre = contract_last(normed_rows, up_weight)
    act_grad = contract_last(grad_rows, down_weight)
    sigmoid_gate = jax.nn.sigmoid(gate_pre)
    silu_gate = gate_pre * sigmoid_gate
    activation = (silu_gate * up_pre).astype(BF16)
    grad_down = contract_first(activation, grad_rows).astype(BF16)[None]
    up_grad = (act_grad * silu_gate).astype(BF16)
    gate_grad = (act_grad * up_pre * sigmoid_gate * (1.0 + gate_pre * (1.0 - sigmoid_gate))).astype(BF16)
    grad_up = contract_first(up_grad, normed_rows).astype(BF16)[None]
    partial_value = jnp.dot(gate_grad, gate_weight, preferred_element_type=F32) + jnp.dot(
        up_grad, up_weight, preferred_element_type=F32
    )
    head_count = entry_state.shape[1]
    head_dim = entry_state.shape[-1]
    survive_here = jnp.exp(jnp.sum(log_decay, axis=1))
    survive_tile = jnp.zeros((8, 128), F32).at[0, :head_count].set(survive_here)
    stream_grad, stream_full, kept_all, survive_all = give_back(
        experts,
        tp_count,
        partial_value.astype(BF16),
        pick,
        mixer_out,
        layer_grad,
        jnp.broadcast_to(row_scale[:, None], (tokens_here, 128)),
        gain_cols[None, :],
        retained,
        survive_tile,
    )
    out_grad = contract_last(stream_full, out_proj).astype(BF16)

    def split_heads(block):
        return block.astype(F32).reshape(tokens_here, head_count, head_dim)

    head_keys = split_heads(key_rows)
    head_values = split_heads(value_rows)
    grad_query, grad_key, grad_value, state_update, survive, falling = span_terms(
        split_heads(query_rows),
        head_keys,
        head_values,
        split_heads(out_grad),
        log_decay,
        entry_state[0],
    )
    spans = jnp.arange(experts)
    here = lax.axis_index("sp")
    between = (spans[None, :] > here) & (spans[None, :] < spans[:, None])
    factors = jnp.where(between[:, :, None], survive_all[None, :, 0, :head_count], 1.0)
    weight = jnp.prod(factors, axis=1) * (spans > here)[:, None]
    per_head = head_dim * head_dim // 128
    weight_rows = jnp.broadcast_to(
        weight[:, :, None, None], (experts, head_count, per_head, 128)
    ).reshape(experts, head_count * per_head, 128)
    cut = stream_full.reshape(tokens_here, experts, -1).transpose(1, 0, 2)
    carried, cols_all = exchange(
        experts, tp_count, state_update.astype(BF16).reshape(head_count * per_head, 128), weight_rows, cut
    )
    grad_key, grad_value = add_carried(
        grad_key, grad_value, head_keys, head_values, falling, carried.reshape(head_count, head_dim, head_dim)
    )
    grad_proj = contract_first(
        cols_all.reshape(-1, cols_all.shape[-1]), kept_all.reshape(-1, kept_all.shape[-1])
    )
    ret_cols = head_count * head_dim
    return (
        grad_up,
        grad_down,
        grad_proj,
        grad_query.reshape(tokens_here, ret_cols).astype(BF16),
        grad_key.reshape(tokens_here, ret_cols).astype(BF16),
        grad_value.reshape(tokens_here, ret_cols).astype(BF16),
        stream_grad,
    )


def solution(mesh):
    in_specs = (
        P("sp", "tp"),
        P("sp", "tp"),
        P("sp"),
        P(),
        P("sp", None),
        P("sp", None),
        P("sp", "tp", None),
        P("sp", "tp", None),
        P("sp", "tp", None),
        P("sp", "tp"),
        P("sp", "tp"),
        P("sp", "tp"),
        P("sp", "tp"),
        P("tp", "sp"),
        P("sp", "tp", None, None),
        P("tp", None),
    )
    out_specs = (
        P("sp", "tp", None),
        P("sp", "tp", None),
        P("sp", "tp"),
        P("sp", "tp"),
        P("sp", "tp"),
        P("sp", "tp"),
        P("sp", "tp"),
    )
    return jax.shard_map(body, mesh=mesh, in_specs=in_specs, out_specs=out_specs, check_vma=False)
```

time: 273 us -> 150 us (0.55); the launches traced: 269 us -> 149 us
  waiting for transfers between devices: 103 us -> 0 us
  Pallas kernels: 0 us -> 97.2 us
  blocking collectives: 86.6 us -> 0 us
  between operations: 15 us -> 1.05 us
  starting transfers between devices: 5.8 us -> 0 us
  local copies, waits for them, and re-layouts: 14.6 us -> 11.3 us
    pallas_call x0 -> x3, Pallas kernels: none -> 97.2 us  [the longest x1 42.1 us: dispatch(): pl.pallas_call(functools.partial(dispatch_kernel, n, tp), out_shape=(full...]
    reduce_scatter x2 -> x0, waiting for transfers between devices: 79.5 us -> none  [the longest x1 64.3 us: body(): lax.psum_scatter(contract_first(stream_full, retained).astype(jnp.bfloat1...]
    all_gather x2 -> x0, blocking collectives: 35.1 us -> none  [the longest x1 27.2 us: prefix(): everything = jax.tree.map(lambda part: lax.all_gather(part, axis), array)]
    all_to_all x2 -> x0, blocking collectives: 34.4 us -> none  [the longest x1 17.4 us: body(): lax.all_to_all(send_grad, 'sp', split_axis=0, concat_axis=0, tiled=True)]
    all_gather x2 -> x0, waiting for transfers between devices: 21.7 us -> none  [the longest x1 14.1 us: body(): lax.all_gather(got_grad, 'tp', axis=2, tiled=True)]
    unnamed x1 -> x0, blocking collectives: 11.6 us -> none
    dot_general x4, matrix products: 16.3 us -> 10.6 us  [contract_last(): lax.dot_general(first_op, second_op, (((1,), (1,)), ((), ())), preferred_...]
    psum x1 -> x0, blocking collectives: 5.59 us -> none  [body(): total_dot = lax.psum(jnp.sum(scaled * attend, axis=1), 'tp')]
  transfers between devices with their start and end apart: 5 -> 0, of which waited for: 5 -> 0; matrix products, arithmetic and copies ran while one was open for 10% -> 0% of each run, Pallas kernels for 0% -> 0%
where the time goes in v1:
time: 150 us; the launch traced here: 149 us
  Pallas kernels  97.2 us (65%)
  matrix products  34.7 us (23%)
  local copies, waits for them, and re-layouts  11.3 us (8%)
  other arithmetic  5.22 us (3%)
    pallas_call x1, Pallas kernels, dispatch(): pl.pallas_call(functools.partial(dispatch_kernel, n, tp), out_shape=(full...  42.1 us
    pallas_call x1, Pallas kernels, give_back(): pl.pallas_call(functools.partial(return_kernel, n, tp), out_shape=(jax.Sh...  35.8 us
    pallas_call x1, Pallas kernels, exchange(): pl.pallas_call(functools.partial(exchange_kernel, n, tp), out_shape=(jax....  19.3 us
    dot_general x5, matrix products, contract_first(): lax.dot_general(first_op, second_op, (((0,), (0,)), ((), ())), preferred_...  15.1 us
    dot_general x4, matrix products, contract_last(): lax.dot_general(first_op, second_op, (((1,), (1,)), ((), ())), preferred_...  10.6 us
    dot_general x1, matrix products, body(): jnp.dot(gate_grad, gate_weight, preferred_element_type=F32)  4.18 us
    unnamed x53, local copies, waits for them, and re-layouts  3.5 us

profile of v1, /device:TPU:11, one launch (start us, length us, event | category | flops | bytes accessed | tf_op | source)
XLA Modules:
  0.0 149.5 jit_solution(13570562744179833337)
XLA Ops:
  0.6 0.0 copy-start
  0.7 0.8 dynamic-slice_convert_fusion
  1.5 0.7 convert_reduce_fusion
  2.2 0.1 convolution_convert_fusion.3
  2.3 0.7 select_reduce_fusion.2
  3.0 0.7 multiply_add_fusion
  3.7 0.1 fusion.26
  3.8 2.1 %convolution_convert_fusion = bf16[512,512]{1,0:T(8,128)(2,1)} fusion(pred[128,512]{1,0:T(8,128)(4,1)S(1)} %fusion.26, bf16[128,512]{1,0:T(8,128)(2,1)} %mixer_ref.1, f32[512]{0:T(512)S(1)} %dynamic-slice_convert_fusion, f32[128]{0:T(128)} %param.20), kind=kOutput, calls=%fused_computation.20 | convolution fusion | flops 67633152 | bytes 723456 | tf_op jit(solution)/shard_map/dot_general | solution.py:352
  5.9 0.8 select_reduce_fusion
  6.7 2.1 %fusion.13 = bf16[512,512]{1,0:T(8,128)(2,1)} fusion(pred[128,512]{1,0:T(8,128)(4,1)S(1)} %fusion.26, bf16[128,512]{1,0:T(8,128)(2,1)} %layer_ref.1, f32[512]{0:T(512)S(1)} %select_reduce_fusion), kind=kOutput, calls=%fused_computation.19 | convolution fusion | flops 67633152 | bytes 722944 | tf_op jit(solution)/shard_map/dot_general | solution.py:352
  8.8 42.1 %dispatch.1 = (bf16[512,2048]{1,0:T(8,128)(2,1)}, bf16[512,2048]{1,0:T(8,128)(2,1)}) custom-call(bf16[8,64,512]{2,1,0:T(8,128)(2,1)} %bitcast.108, bf16[8,64,512]{2,1,0:T(8,128)(2,1)} %bitcast.109), custom_call_target="tpu_custom_call" | custom-call | tf_op jit(solution)/shard_map/dispatch/pallas_call | solution.py:121
  50.9 0.0 copy-start.12
  51.0 5.2 %fusion.6 = f32[512,896]{1,0:T(8,128)S(1)} fusion(bf16[512,2048]{1,0:T(8,128)(2,1)} %get-tuple-element.28, bf16[1,896,2048]{2,1,0:T(8,128)(2,1)} %param.24), kind=kOutput, calls=%fused_computation.7 | convolution fusion | flops 1879048192 | bytes 7602176 | tf_op jit(solution)/shard_map/dot_general | solution.py:346
  56.2 2.5 %multiply_convert_fusion.2 = (bf16[512,896]{1,0:T(8,128)(2,1)S(1)}, f32[512,896]{1,0:T(8,128)S(1)}) fusion(f32[512,896]{1,0:T(8,128)S(1)} %fusion.6, bf16[512,2048]{1,0:T(8,128)(2,1)S(1)} %copy-done.15, bf16[1,896,2048]{2,1,0:T(8,128)(2,1)S(1)} %copy-done.12), kind=kOutput, calls=%fused_computation.15 | convolution fusion | flops 1881800704 | bytes 10354688 | tf_op jit(solution)/shard_map/dot_general | solution.py:346
  58.7 0.1 copy-done.13
  58.9 2.4 %fusion = f32[512,2048]{1,0:T(8,128)S(1)} fusion(bf16[512,896]{1,0:T(8,128)(2,1)S(1)} %get-tuple-element.58, bf16[1,896,2048]{2,1,0:T(8,128)(2,1)S(1)} %copy-done.13), kind=kOutput, calls=%fused_computation.1 | convolution fusion | flops 1879048192 | bytes 8781824 | tf_op jit(solution)/shard_map/dot_general | solution.py:460
  61.3 0.0 copy-start.14
  61.3 2.4 %fusion.2 = f32[512,896]{1,0:T(8,128)S(1)} fusion(bf16[512,2048]{1,0:T(8,128)(2,1)S(1)} %copy-done.17, bf16[1,896,2048]{2,1,0:T(8,128)(2,1)S(1)} %copy-done.13), kind=kOutput, calls=%fused_computation.3 | convolution fusion | flops 1879048192 | bytes 7602176 | tf_op jit(solution)/shard_map/dot_general | solution.py:346
  63.7 0.0 copy-start.11
  63.7 0.0 copy-start.10
  63.7 4.2 %add_convert_fusion.part_ref = bf16[512,2048]{1,0:T(8,128)(2,1)} fusion(f32[512,2048]{1,0:T(8,128)S(1)} %fusion, bf16[1,896,2048]{2,1,0:T(8,128)(2,1)S(1)} %copy-done.14, f32[512,896]{1,0:T(8,128)S(1)} %fusion.6, f32[512,896]{1,0:T(8,128)S(1)} %get-tuple-element.59, f32[512,896]{1,0:T(8,128)S(1)} %fusion.2), kind=kOutput, calls=%fused_computation | convolution fusion | flops 1885732864 | bytes 15466496 | tf_op jit(solution)/shard_map/dot_general | solution.py:460
  67.9 0.7 convert_element_type.96.pick_ref
  68.6 0.7 broadcast_in_dim.121.scale_ref
  69.3 0.1 reduce_sum.39
  69.4 0.6 scatter.4.surv_ref
  70.0 35.8 %give_back.1 = (bf16[128,512]{1,0:T(8,128)(2,1)}, bf16[128,2048]{1,0:T(8,128)(2,1)}, bf16[8,128,256]{2,1,0:T(8,128)(2,1)}, f32[8,8,128]{2,1,0:T(8,128)}) custom-call(bf16[512,2048]{1,0:T(8,128)(2,1)} %add_convert_fusion.part_ref, bf16[128,512]{1,0:T(8,128)(2,1)} %convert_element_type.96.pick_ref, bf16[128,512]{1,0:T(8,128)(2,1)} %mixer_ref.1, ...), custom_call_target="tpu_custom_call" | custom-call | tf_op jit(solution)/shard_map/give_back/pallas_call | solution.py:256
  105.8 1.4 copy.65
  107.2 1.0 copy.66
  108.2 0.8 slice.22
  109.0 0.1 copy.63
  109.1 0.1 select_reduce_fusion.1
  109.3 0.1 copy.64
  109.4 0.1 broadcast_in_dim.127
  109.4 0.1 broadcast_in_dim.128
  109.5 1.0 broadcast_in_dim.129.weight_ref
  110.5 0.5 convolution_convert_fusion.1
  111.0 0.0 copy-start.8
  111.1 0.1 copy.62
  111.2 0.3 reduce_window_sum.11
  111.5 0.2 slice_reduce_fusion
  111.7 0.1 multiply_bitcast_fusion
  111.7 0.1 copy.61
  111.9 0.2 convolution_convert_fusion.2
  112.1 0.7 reshape.173.state_ref
  112.8 19.3 %exchange.1 = (f32[128,128]{1,0:T(8,128)}, bf16[8,128,256]{2,1,0:T(8,128)(2,1)}) custom-call(bf16[128,128]{1,0:T(8,128)(2,1)} %reshape.173.state_ref, f32[8,128,128]{2,1,0:T(8,128)} %broadcast_in_dim.129.weight_ref, bf16[8,128,256]{2,1,0:T(8,128)(2,1)} %bitcast.107), custom_call_target="tpu_custom_call" | custom-call | tf_op jit(solution)/shard_map/exchange/pallas_call | solution.py:330
  132.2 0.0 copy-start.4
  132.2 1.0 reshape.177
  133.1 0.1 copy.69
  133.3 0.3 fusion.16
  133.6 0.2 fusion.14
  133.9 0.3 fusion.22
  134.1 0.7 copy.73
  134.9 0.1 copy.68
  135.0 0.2 fusion.17
  135.2 0.2 fusion.15
  135.4 0.2 fusion.23
  135.7 0.7 copy.72
  136.4 0.2 fusion.18
  136.7 0.4 fusion.24
  137.0 0.7 copy.71
  137.8 1.0 convolution_bitcast_fusion
  138.8 6.0 %convert_bitcast_fusion.1 = bf16[1,896,2048]{2,1,0:T(8,128)(2,1)} fusion(bf16[512,896]{1,0:T(8,128)(2,1)} %copy-done.22, bf16[512,2048]{1,0:T(8,128)(2,1)} %get-tuple-element.28), kind=kOutput, calls=%fused_computation.12 | convolution fusion | flops 1880883200 | bytes 6684672 | tf_op jit(solution)/shard_map/dot_general | solution.py:352
  144.8 4.0 %convert_bitcast_fusion = bf16[1,896,2048]{2,1,0:T(8,128)(2,1)} fusion(bf16[512,2048]{1,0:T(8,128)(2,1)S(1)} %copy-done.16, f32[512,896]{1,0:T(8,128)S(1)} %copy-done.21, f32[512,896]{1,0:T(8,128)S(1)} %copy-done.19), kind=kOutput, calls=%fused_computation.11 | convolution fusion | flops 1883635712 | bytes 9437184 | tf_op jit(solution)/shard_map/dot_general | solution.py:352
  148.8 0.7 copy.77
  (44 shorter events, 0.1 us)
Async XLA Ops:
  0.6 109.9 %copy-start = (bf16[256,2048]{1,0:T(8,128)(2,1)S(1)}, bf16[256,2048]{1,0:T(8,128)(2,1)}, u32[]{:S(2)}) copy-start(bf16[256,2048]{1,0:T(8,128)(2,1)} %param.33) | copy-start | bytes 3145732
  1.5 54.7 %copy-start.9 = (f32[512]{0:T(512)}, f32[512]{0:T(512)S(1)}, u32[]{:S(2)}) copy-start(f32[512]{0:T(512)S(1)} %dynamic-slice_convert_fusion) | copy-start | bytes 6148
  50.9 5.2 %copy-start.12 = (bf16[1,896,2048]{2,1,0:T(8,128)(2,1)S(1)}, bf16[1,896,2048]{2,1,0:T(8,128)(2,1)}, u32[]{:S(2)}) copy-start(bf16[1,896,2048]{2,1,0:T(8,128)(2,1)} %param.26) | copy-start | bytes 11010052
  51.0 5.2 %copy-start.15 = (bf16[512,2048]{1,0:T(8,128)(2,1)S(1)}, bf16[512,2048]{1,0:T(8,128)(2,1)}, u32[]{:S(2)}) copy-start(bf16[512,2048]{1,0:T(8,128)(2,1)} %get-tuple-element.27) | copy-start | bytes 6291460
  56.2 7.5 %copy-start.18 = (f32[512,896]{1,0:T(8,128)}, f32[512,896]{1,0:T(8,128)S(1)}, u32[]{:S(2)}) copy-start(f32[512,896]{1,0:T(8,128)S(1)} %fusion.6) | copy-start | bytes 5505028
  56.2 2.7 %copy-start.13 = (bf16[1,896,2048]{2,1,0:T(8,128)(2,1)S(1)}, bf16[1,896,2048]{2,1,0:T(8,128)(2,1)}, u32[]{:S(2)}) copy-start(bf16[1,896,2048]{2,1,0:T(8,128)(2,1)} %param.25) | copy-start | bytes 11010052
  58.7 2.6 %copy-start.22 = (bf16[512,896]{1,0:T(8,128)(2,1)}, bf16[512,896]{1,0:T(8,128)(2,1)S(1)}, u32[]{:S(2)}) copy-start(bf16[512,896]{1,0:T(8,128)(2,1)S(1)} %get-tuple-element.58) | copy-start | bytes 2752516
  58.9 2.4 %copy-start.17 = (bf16[512,2048]{1,0:T(8,128)(2,1)S(1)}, bf16[512,2048]{1,0:T(8,128)(2,1)}, u32[]{:S(2)}) copy-start(bf16[512,2048]{1,0:T(8,128)(2,1)} %get-tuple-element.28) | copy-start | bytes 6291460
  61.3 2.4 %copy-start.14 = (bf16[1,896,2048]{2,1,0:T(8,128)(2,1)S(1)}, bf16[1,896,2048]{2,1,0:T(8,128)(2,1)}, u32[]{:S(2)}) copy-start(bf16[1,896,2048]{2,1,0:T(8,128)(2,1)} %param.24) | copy-start | bytes 11010052
  63.7 4.2 %copy-start.20 = (f32[512,896]{1,0:T(8,128)}, f32[512,896]{1,0:T(8,128)S(1)}, u32[]{:S(2)}) copy-start(f32[512,896]{1,0:T(8,128)S(1)} %fusion.2) | copy-start | bytes 5505028
  63.7 4.9 %copy-start.11 = (f32[128]{0:T(128)S(1)}, f32[128]{0:T(128)}, u32[]{:S(2)}) copy-start(f32[128]{0:T(128)} %param.20) | copy-start | bytes 1540
  63.7 5.6 %copy-start.10 = (f32[4,128]{1,0:T(4,128)S(1)}, f32[4,128]{1,0:T(4,128)}, u32[]{:S(2)}) copy-start(f32[4,128]{1,0:T(4,128)} %param.31) | copy-start | bytes 6148
  105.8 4.7 %copy-start.1 = (bf16[128,2048]{1,0:T(8,128)(2,1)S(1)}, bf16[128,2048]{1,0:T(8,128)(2,1)}, u32[]{:S(2)}) copy-start(bf16[128,2048]{1,0:T(8,128)(2,1)} %get-tuple-element.29) | copy-start | bytes 1572868
  105.8 5.9 %copy-start.6 = (bf16[128,256]{1,0:T(8,128)(2,1)S(1)}, bf16[128,256]{1,0:T(8,128)(2,1)}, u32[]{:S(2)}) copy-start(bf16[128,256]{1,0:T(8,128)(2,1)} %param.27) | copy-start | bytes 196612
  108.2 24.9 %copy-start.7 = (bf16[128,256]{1,0:T(8,128)(2,1)S(1)}, bf16[128,256]{1,0:T(8,128)(2,1)}, u32[]{:S(2)}) copy-start(bf16[128,256]{1,0:T(8,128)(2,1)} %param.28) | copy-start | bytes 196612
  111.0 23.8 %copy-start.8 = (bf16[128,256]{1,0:T(8,128)(2,1)S(1)}, bf16[128,256]{1,0:T(8,128)(2,1)}, u32[]{:S(2)}) copy-start(bf16[128,256]{1,0:T(8,128)(2,1)} %param.29) | copy-start | bytes 196612
  132.2 4.3 %copy-start.4 = (f32[1,4,64,64]{3,2,1,0:T(8,128)S(1)}, f32[1,4,64,64]{3,2,1,0:T(8,128)}, u32[]{:S(2)}) copy-start(f32[1,4,64,64]{3,2,1,0:T(8,128)} %param.32) | copy-start | bytes 196612
  133.6 4.2 %copy-start.2 = (bf16[8,128,256]{2,1,0:T(8,128)(2,1)S(1)}, bf16[8,128,256]{2,1,0:T(8,128)(2,1)}, u32[]{:S(2)}) copy-start(bf16[8,128,256]{2,1,0:T(8,128)(2,1)} %get-tuple-element.32) | copy-start | bytes 1572868
  133.6 4.2 %copy-start.3 = (bf16[8,128,256]{2,1,0:T(8,128)(2,1)S(1)}, bf16[8,128,256]{2,1,0:T(8,128)(2,1)}, u32[]{:S(2)}) copy-start(bf16[8,128,256]{2,1,0:T(8,128)(2,1)} %get-tuple-element.31) | copy-start | bytes 1572868
  138.8 6.0 %copy-start.16 = (bf16[512,2048]{1,0:T(8,128)(2,1)S(1)}, bf16[512,2048]{1,0:T(8,128)(2,1)}, u32[]{:S(2)}) copy-start(bf16[512,2048]{1,0:T(8,128)(2,1)} %get-tuple-element.27) | copy-start | bytes 6291460
  138.8 6.0 %copy-start.19 = (f32[512,896]{1,0:T(8,128)S(1)}, f32[512,896]{1,0:T(8,128)}, u32[]{:S(2)}) copy-start(f32[512,896]{1,0:T(8,128)} %copy-done.18) | copy-start | bytes 5505028
  138.8 6.0 %copy-start.21 = (f32[512,896]{1,0:T(8,128)S(1)}, f32[512,896]{1,0:T(8,128)}, u32[]{:S(2)}) copy-start(f32[512,896]{1,0:T(8,128)} %copy-done.20) | copy-start | bytes 5505028
  144.8 4.0 %copy-start.5 = (bf16[128,512]{1,0:T(8,128)(2,1)S(1)}, bf16[128,512]{1,0:T(8,128)(2,1)}, u32[]{:S(2)}) copy-start(bf16[128,512]{1,0:T(8,128)(2,1)} %get-tuple-element.75) | copy-start | bytes 393220

commit v2 on v1

--- a/solution.py
+++ b/solution.py
@@ -1,4 +1,5 @@
 import functools
+import math
 
 import jax
 import jax.numpy as jnp
@@ -56,9 +57,13 @@
         return [(self.s, self.to_y(k)) for k in range(1, self.rows)] + [self.twin]
 
 
-def dispatch_kernel(n, tp, normed_ref, grad_ref, full_n_ref, full_g_ref, buf, s1, r1, s2, r2, s3, r3):
+def dispatch_kernel(n, tp, normed_ref, grad_ref, gate_ref, up_ref, full_n_ref, full_g_ref, gate_pre_ref, up_pre_ref,
+                    buf, held, wsem, s1, r1, s2, r2, s3, r3):
     at = Place(n, tp)
     capacity, columns = normed_ref.shape[1:]
+    loads = [pltpu.make_async_copy(ref, held.at[i], wsem.at[i]) for i, ref in enumerate((gate_ref, up_ref))]
+    for load in loads:
+        load.start()
     greet(at.sp_peers() + at.y_peers())
     inputs = (normed_ref, grad_ref)
     pending = []
@@ -87,6 +92,28 @@
             start(remote(inputs[kind].at[there], buf.at[kind, at.t, at.s], s1.at[kind, there],
                          r1.at[kind, at.s], (there, at.t)))
         buf[kind, at.t, at.s] = inputs[kind][at.s]
+
+    def complete(kind, out):
+        for k in range(n):
+            source = at.from_sp(k)
+            for hop in range(at.rows):
+                owner = at.twin_t if hop == 0 else lax.rem(at.from_y(hop) + 1 - 2 * at.core, tp)
+                slot = buf.at[kind, owner, source]
+                remote(slot, slot, s3.at[kind, hop, source], r3.at[kind, hop, source], at.twin).wait_recv()
+        for t in range(tp):
+            out[:, t * columns:(t + 1) * columns] = buf[kind, t].reshape(n * capacity, columns)
+
+    hidden = gate_ref.shape[0]
+    tile = math.gcd(hidden, 128)
+    tiles = [(i, j) for j in range(hidden // tile) for i in range(2)]
+    share = -(-len(tiles) // (n - 3))
+
+    def work(count):
+        for i, j in tiles[:count]:
+            rows = slice(j * tile, (j + 1) * tile)
+            (gate_pre_ref, up_pre_ref)[i][rows, :] = contract_last(held[i, rows, :], full_n_ref[...])
+        del tiles[:count]
+
     lag = [(kind, at.s) for kind in range(2)]
     for kind in range(2):
         for k in range(1, n):
@@ -97,41 +124,42 @@
             lag.append((kind, source))
             if len(lag) > 3:
                 hand_on(*lag.pop(0))
+            if kind == 1 and k == 3:
+                complete(0, full_n_ref)
+                for load in loads:
+                    load.wait()
+            if kind == 1 and k >= 3:
+                work(share)
     for item in lag:
         hand_on(*item)
-    for kind in range(2):
-        for k in range(n):
-            source = at.from_sp(k)
-            for hop in range(at.rows):
-                owner = at.twin_t if hop == 0 else lax.rem(at.from_y(hop) + 1 - 2 * at.core, tp)
-                slot = buf.at[kind, owner, source]
-                remote(slot, slot, s3.at[kind, hop, source], r3.at[kind, hop, source], at.twin).wait_recv()
-    for kind, out in enumerate((full_n_ref, full_g_ref)):
-        for t in range(tp):
-            out[:, t * columns:(t + 1) * columns] = buf[kind, t].reshape(n * capacity, columns)
+    work(len(tiles))
+    complete(1, full_g_ref)
     for copy in pending:
         copy.wait_send()
 
 
-def dispatch(n, tp, send_normed, send_grad):
+def dispatch(n, tp, send_normed, send_grad, gate, up):
     _, capacity, columns = send_normed.shape
     rows = tp // 2
     full = jax.ShapeDtypeStruct((n * capacity, tp * columns), BF16)
+    pre = jax.ShapeDtypeStruct((gate.shape[0], n * capacity), F32)
     dma = pltpu.SemaphoreType.DMA
     return pl.pallas_call(
         functools.partial(dispatch_kernel, n, tp),
-        out_shape=(full, full),
-        in_specs=[VMEM] * 2,
-        out_specs=(VMEM, VMEM),
+        out_shape=(full, full, pre, pre),
+        in_specs=[VMEM] * 2 + [pl.BlockSpec(memory_space=pl.ANY)] * 2,
+        out_specs=(VMEM,) * 4,
         scratch_shapes=[
             pltpu.VMEM((2, tp, n, capacity, columns), BF16),
+            pltpu.VMEM((2,) + gate.shape, BF16),
+            dma((2,)),
             dma((2, n)), dma((2, n)),
             dma((2, rows, n)), dma((2, rows, n)),
             dma((2, rows, n)), dma((2, rows, n)),
         ],
         compiler_params=pltpu.CompilerParams(collective_id=1, has_side_effects=True),
         name="dispatch",
-    )(send_normed, send_grad)
+    )(send_normed, send_grad, gate, up)
 
 
 def eye(size):
@@ -139,7 +167,8 @@
 
 
 def return_kernel(n, tp, part_ref, pick_ref, mixer_ref, layer_ref, scale_ref, gain_ref, kept_ref, surv_ref,
-                  stream_ref, full_ref, kept_all_ref, surv_all_ref,
+                  act_ref, up_grad_ref, grad_rows_ref, normed_rows_ref,
+                  stream_ref, full_ref, kept_all_ref, surv_all_ref, grad_down_ref, grad_up_ref,
                   b1, s1buf, b2, total, back, stat, sbuf,
                   sa, ra, sb, rb, sc, rc, sd, rd, se, re, sf, rf, sk, rk, sv, rv):
     at = Place(n, tp)
@@ -185,7 +214,21 @@
             s1buf[k - 1, block] = mine(block, yy).astype(BF16)
             start(remote(s1buf.at[k - 1, block], b2.at[k - 1, block], sb.at[k - 1, block],
                          rb.at[k - 1, block], (at.s, at.to_y(k))))
+    hidden_units = act_ref.shape[0]
+    tile = math.gcd(hidden_units, 128)
+    tiles = [(i, j) for i in range(2) for j in range(hidden_units // tile)]
+    share = -(-len(tiles) // n)
+
+    def work(count):
+        for i, j in tiles[:count]:
+            rows = slice(j * tile, (j + 1) * tile)
+            left, right, out = (
+                (act_ref, grad_rows_ref, grad_down_ref), (up_grad_ref, normed_rows_ref, grad_up_ref))[i]
+            out[rows, :] = jnp.dot(left[rows, :], right[...], preferred_element_type=F32).astype(BF16)
+        del tiles[:count]
+
     for place, block in enumerate(order):
+        work(share)
         summed = mine(block, at.y)
         for k in range(1, at.rows):
             slot = b2.at[k - 1, block]
@@ -249,7 +292,7 @@
         copy.wait_send()
 
 
-def give_back(n, tp, part, pick, mixer, layer, row_scale, gain, kept, surv):
+def give_back(n, tp, part, pick, mixer, layer, row_scale, gain, kept, surv, act, up_grad, grad_rows, normed_rows):
     tokens, columns = mixer.shape
     rows, capacity = tp // 2, part.shape[0] // n
     dma = pltpu.SemaphoreType.DMA
@@ -260,9 +303,11 @@
             jax.ShapeDtypeStruct((tokens, tp * columns), BF16),
             jax.ShapeDtypeStruct((n,) + kept.shape, BF16),
             jax.ShapeDtypeStruct((n,) + surv.shape, F32),
+            jax.ShapeDtypeStruct((act.shape[0], tp * columns), BF16),
+            jax.ShapeDtypeStruct((act.shape[0], tp * columns), BF16),
         ),
-        in_specs=[VMEM] * 8,
-        out_specs=(VMEM,) * 4,
+        in_specs=[VMEM] * 12,
+        out_specs=(VMEM,) * 6,
         scratch_shapes=[
             pltpu.VMEM((rows, n * capacity, columns), BF16),
             pltpu.VMEM((rows, n, capacity, columns), BF16),
@@ -282,7 +327,7 @@
         ],
         compiler_params=pltpu.CompilerParams(collective_id=2, has_side_effects=True),
         name="give_back",
-    )(part, pick, mixer, layer, row_scale, gain, kept, surv)
+    )(part, pick, mixer, layer, row_scale, gain, kept, surv, act, up_grad, grad_rows, normed_rows)
 
 
 def exchange_kernel(n, tp, state_ref, weight_ref, cut_ref, carried_ref, cols_ref, sbuf, cbuf, su, ru, sc, rc, sd, rd):
@@ -443,28 +488,24 @@
     send_grad = (slot_weight[:, None] * contract_first(pick, layer_grad)).astype(BF16).reshape(
         experts, capacity, columns
     )
-    normed_rows, grad_rows = dispatch(experts, tp_count, send_normed, send_grad)
     gate_weight = expert_gate[0]
     up_weight = expert_up[0]
     down_weight = expert_down[0]
-    gate_pre = contract_last(normed_rows, gate_weight)
-    up_pre = contract_last(normed_rows, up_weight)
-    act_grad = contract_last(grad_rows, down_weight)
+    normed_rows, grad_rows, gate_pre, up_pre = dispatch(
+        experts, tp_count, send_normed, send_grad, gate_weight, up_weight
+    )
+    act_grad = contract_last(down_weight, grad_rows)
     sigmoid_gate = jax.nn.sigmoid(gate_pre)
     silu_gate = gate_pre * sigmoid_gate
     activation = (silu_gate * up_pre).astype(BF16)
-    grad_down = contract_first(activation, grad_rows).astype(BF16)[None]
     up_grad = (act_grad * silu_gate).astype(BF16)
     gate_grad = (act_grad * up_pre * sigmoid_gate * (1.0 + gate_pre * (1.0 - sigmoid_gate))).astype(BF16)
-    grad_up = contract_first(up_grad, normed_rows).astype(BF16)[None]
-    partial_value = jnp.dot(gate_grad, gate_weight, preferred_element_type=F32) + jnp.dot(
-        up_grad, up_weight, preferred_element_type=F32
-    )
+    partial_value = contract_first(gate_grad, gate_weight) + contract_first(up_grad, up_weight)
     head_count = entry_state.shape[1]
     head_dim = entry_state.shape[-1]
     survive_here = jnp.exp(jnp.sum(log_decay, axis=1))
     survive_tile = jnp.zeros((8, 128), F32).at[0, :head_count].set(survive_here)
-    stream_grad, stream_full, kept_all, survive_all = give_back(
+    stream_grad, stream_full, kept_all, survive_all, grad_down, grad_up = give_back(
         experts,
         tp_count,
         partial_value.astype(BF16),
@@ -475,6 +516,10 @@
         gain_cols[None, :],
         retained,
         survive_tile,
+        activation,
+        up_grad,
+        grad_rows,
+        normed_rows,
     )
     out_grad = contract_last(stream_full, out_proj).astype(BF16)
 
@@ -512,8 +557,8 @@
     )
     ret_cols = head_count * head_dim
     return (
-        grad_up,
-        grad_down,
+        grad_up[None],
+        grad_down[None],
         grad_proj,
         grad_query.reshape(tokens_here, ret_cols).astype(BF16),
         grad_key.reshape(tokens_here, ret_cols).astype(BF16),

time: 150 us -> 154 us (1.027)
  matrix products: 34.7 us -> 22.1 us
  Pallas kernels: 97.2 us -> 107 us
  local copies, waits for them, and re-layouts: 11.3 us -> 17.5 us
    dot_general x2 -> x0, matrix products: 6.56 us -> none  [the longest x1 4.18 us: body(): jnp.dot(gate_grad, gate_weight, preferred_element_type=F32)]
    unnamed x53 -> x45, local copies, waits for them, and re-layouts: 3.5 us -> 9.69 us
    pallas_call x1, Pallas kernels: 35.8 us -> 41.3 us  [give_back(): pl.pallas_call(functools.partial(return_kernel, n, tp), out_shape=(jax.Sh...]
    pallas_call x1, Pallas kernels: 42.1 us -> 46.7 us  [dispatch(): pl.pallas_call(functools.partial(dispatch_kernel, n, tp), out_shape=(full...]
    dot_general x5, matrix products: 15.1 us -> 12 us  [contract_first(): lax.dot_general(first_op, second_op, (((0,), (0,)), ((), ())), preferred_...]
    dot_general x4 -> x2, matrix products: 10.6 us -> 7.68 us  [contract_last(): lax.dot_general(first_op, second_op, (((1,), (1,)), ((), ())), preferred_...]
where the time goes in v2:
time: 154 us; the launch traced here: 153 us
  Pallas kernels  107 us (69%)
  matrix products  22.1 us (14%)
  local copies, waits for them, and re-layouts  17.5 us (11%)
  other arithmetic  5.22 us (3%)
    pallas_call x1, Pallas kernels, dispatch(): pl.pallas_call(functools.partial(dispatch_kernel, n, tp), out_shape=(full...  46.7 us
    pallas_call x1, Pallas kernels, give_back(): pl.pallas_call(functools.partial(return_kernel, n, tp), out_shape=(jax.Sh...  41.3 us
    pallas_call x1, Pallas kernels, exchange(): pl.pallas_call(functools.partial(exchange_kernel, n, tp), out_shape=(jax....  19.3 us
    dot_general x5, matrix products, contract_first(): lax.dot_general(first_op, second_op, (((0,), (0,)), ((), ())), preferred_...  12 us
    unnamed x45, local copies, waits for them, and re-layouts  9.69 us
    dot_general x2, matrix products, contract_last(): lax.dot_general(first_op, second_op, (((1,), (1,)), ((), ())), preferred_...  7.68 us

profile of v2, /device:TPU:11, one launch (start us, length us, event | category | flops | bytes accessed | tf_op | source)
XLA Modules:
  0.0 153.2 jit_solution(6926874381343836849)
XLA Ops:
  0.6 0.0 copy-start
  0.7 0.8 dynamic-slice_convert_fusion
  1.5 0.7 convert_reduce_fusion
  2.2 0.1 convolution_convert_fusion.3
  2.3 0.7 select_reduce_fusion.2
  3.0 0.7 multiply_add_fusion
  3.7 0.1 fusion.22
  3.8 2.1 %convolution_convert_fusion = bf16[512,512]{1,0:T(8,128)(2,1)} fusion(pred[128,512]{1,0:T(8,128)(4,1)S(1)} %fusion.22, bf16[128,512]{1,0:T(8,128)(2,1)} %mixer_ref.1, f32[512]{0:T(512)S(1)} %dynamic-slice_convert_fusion, f32[128]{0:T(128)} %param.20), kind=kOutput, calls=%fused_computation.14 | convolution fusion | flops 67633152 | bytes 723456 | tf_op jit(solution)/shard_map/dot_general | solution.py:397
  5.9 0.8 select_reduce_fusion
  6.7 2.1 %fusion.7 = bf16[512,512]{1,0:T(8,128)(2,1)} fusion(pred[128,512]{1,0:T(8,128)(4,1)S(1)} %fusion.22, bf16[128,512]{1,0:T(8,128)(2,1)} %layer_ref.1, f32[512]{0:T(512)S(1)} %select_reduce_fusion), kind=kOutput, calls=%fused_computation.13 | convolution fusion | flops 67633152 | bytes 722944 | tf_op jit(solution)/shard_map/dot_general | solution.py:397
  8.8 46.7 %dispatch.1 = (bf16[512,2048]{1,0:T(8,128)(2,1)}, bf16[512,2048]{1,0:T(8,128)(2,1)}, f32[896,512]{1,0:T(8,128)}, f32[896,512]{1,0:T(8,128)}) custom-call(bf16[8,64,512]{2,1,0:T(8,128)(2,1)} %bitcast.110, bf16[8,64,512]{2,1,0:T(8,128)(2,1)} %bitcast.111, bf16[896,2048]{1,0:T(8,128)(2,1)} %bitcast.109, bf16[896,2048]{1,0:T(8,128)(2,1)} %bitcast.106), custom_call_target="tpu_custom_call" | custom-call | tf_op jit(solution)/shard_map/dispatch/pallas_call | solution.py:147
  55.5 0.0 copy-done.13
  55.6 0.0 copy-start.4
  55.6 7.2 %multiply_convert_fusion = (bf16[896,512]{1,0:T(8,128)(2,1)}, bf16[896,512]{1,0:T(8,128)(2,1)S(1)}, f32[512,896]{0,1:T(8,128)S(1)}) fusion(f32[896,512]{1,0:T(8,128)} %get-tuple-element.32, f32[896,512]{1,0:T(8,128)} %get-tuple-element.33, bf16[512,2048]{1,0:T(8,128)(2,1)} %get-tuple-element.31.grad_rows_ref, bf16[1,896,2048]{2,1,0:T(8,128)(2,1)} %param.26), kind=kOutput, calls=%fused_computation.9 | convolution fusion | flops 1882718208 | bytes 13107200 | tf_op jit(solution)/shard_map/dot_general | solution.py:391
  62.8 0.0 copy-done.16
  62.8 0.0 copy-start.1
  62.8 3.0 %fusion.19 = f32[512,2048]{1,0:T(8,128)S(1)} fusion(f32[896,512]{1,0:T(8,128)S(1)} %copy-done.17, f32[512,896]{0,1:T(8,128)S(1)} %get-tuple-element.68, f32[896,512]{1,0:T(8,128)S(1)} %copy-done.16, bf16[1,896,2048]{2,1,0:T(8,128)(2,1)S(1)} %copy-done.4), kind=kOutput, calls=%fused_computation.38 | convolution fusion | flops 1883635712 | bytes 13369344 | tf_op jit(solution)/shard_map/dot_general | solution.py:397
  65.8 0.0 copy-start.15
  65.8 0.0 copy-start.14
  65.8 3.9 %add_convert_fusion.part_ref = bf16[512,2048]{1,0:T(8,128)(2,1)} fusion(f32[512,2048]{1,0:T(8,128)S(1)} %fusion.19, bf16[896,512]{1,0:T(8,128)(2,1)S(1)} %get-tuple-element.65.up_grad_ref, bf16[1,896,2048]{2,1,0:T(8,128)(2,1)S(1)} %copy-done.1), kind=kOutput, calls=%fused_computation | convolution fusion | flops 1881145344 | bytes 10878976 | tf_op jit(solution)/shard_map/dot_general | solution.py:397
  69.7 0.7 convert_element_type.87.pick_ref
  70.4 0.7 broadcast_in_dim.119.scale_ref
  71.1 0.1 reduce_sum.39
  71.2 0.6 scatter.4.surv_ref
  71.8 41.3 %give_back.1 = (bf16[128,512]{1,0:T(8,128)(2,1)}, bf16[128,2048]{1,0:T(8,128)(2,1)}, bf16[8,128,256]{2,1,0:T(8,128)(2,1)}, f32[8,8,128]{2,1,0:T(8,128)}, bf16[89...) custom-call(bf16[512,2048]{1,0:T(8,128)(2,1)} %add_convert_fusion.part_ref, ...), custom_call_target="tpu_custom_call" | custom-call | tf_op jit(solution)/shard_map/give_back/pallas_call | solution.py:299
  113.2 1.4 copy.68
  114.6 0.0 copy-start.10
  114.6 1.0 copy.69
  115.6 0.8 slice.22
  116.4 0.1 copy.66
  116.5 0.1 select_reduce_fusion.1
  116.6 0.1 copy.67
  116.7 0.1 broadcast_in_dim.127
  116.8 0.1 broadcast_in_dim.128
  116.9 1.0 broadcast_in_dim.129.weight_ref
  117.9 0.5 convolution_convert_fusion.1
  118.4 0.0 copy-start.12
  118.4 0.1 copy.65
  118.5 0.3 reduce_window_sum.11
  118.8 0.2 slice_reduce_fusion
  119.0 0.1 multiply_bitcast_fusion
  119.1 0.1 copy.64
  119.2 0.2 convolution_convert_fusion.2
  119.5 0.7 reshape.173.state_ref
  120.2 19.3 %exchange.1 = (f32[128,128]{1,0:T(8,128)}, bf16[8,128,256]{2,1,0:T(8,128)(2,1)}) custom-call(bf16[128,128]{1,0:T(8,128)(2,1)} %reshape.173.state_ref, f32[8,128,128]{2,1,0:T(8,128)} %broadcast_in_dim.129.weight_ref, bf16[8,128,256]{2,1,0:T(8,128)(2,1)} %bitcast.112), custom_call_target="tpu_custom_call" | custom-call | tf_op jit(solution)/shard_map/exchange/pallas_call | solution.py:375
  139.5 0.0 copy-start.8
  139.5 1.0 reshape.177
  140.5 0.1 copy.72
  140.6 0.3 fusion.10
  140.9 0.2 fusion.8
  141.2 0.3 fusion.16
  141.4 0.7 copy.76
  142.2 0.1 copy.71
  142.3 0.2 fusion.11
  142.5 0.2 fusion.9
  142.8 0.2 fusion.17
  143.0 0.7 copy.75
  143.8 0.2 fusion.12
  144.0 0.4 fusion.18
  144.4 0.7 copy.74
  145.1 1.0 convolution_bitcast_fusion
  146.2 4.5 %copy.83 = bf16[1,896,2048]{2,1,0:T(8,128)(2,1)} copy(bf16[1,896,2048]{2,1,0:T(8,128)(2,1)} %bitcast.108) | data formatting | bytes 7340032
  150.7 1.8 %copy.84 = bf16[1,896,2048]{2,1,0:T(8,128)(2,1)} copy(bf16[1,896,2048]{2,1,0:T(8,128)(2,1)S(1)} %bitcast.107) | data formatting | bytes 7340032
  152.5 0.7 copy.85
  (32 shorter events, 0.1 us)
Async XLA Ops:
  0.6 117.2 %copy-start = (bf16[256,2048]{1,0:T(8,128)(2,1)S(1)}, bf16[256,2048]{1,0:T(8,128)(2,1)}, u32[]{:S(2)}) copy-start(bf16[256,2048]{1,0:T(8,128)(2,1)} %param.33) | copy-start | bytes 3145732
  1.5 54.0 %copy-start.13 = (f32[512]{0:T(512)}, f32[512]{0:T(512)S(1)}, u32[]{:S(2)}) copy-start(f32[512]{0:T(512)S(1)} %dynamic-slice_convert_fusion) | copy-start | bytes 6148
  55.6 7.2 %copy-start.4 = (bf16[1,896,2048]{2,1,0:T(8,128)(2,1)S(1)}, bf16[1,896,2048]{2,1,0:T(8,128)(2,1)}, u32[]{:S(2)}) copy-start(bf16[1,896,2048]{2,1,0:T(8,128)(2,1)} %param.24) | copy-start | bytes 11010052
  55.6 7.2 %copy-start.16 = (f32[896,512]{1,0:T(8,128)S(1)}, f32[896,512]{1,0:T(8,128)}, u32[]{:S(2)}) copy-start(f32[896,512]{1,0:T(8,128)} %get-tuple-element.33) | copy-start | bytes 5505028
  55.6 7.2 %copy-start.17 = (f32[896,512]{1,0:T(8,128)S(1)}, f32[896,512]{1,0:T(8,128)}, u32[]{:S(2)}) copy-start(f32[896,512]{1,0:T(8,128)} %get-tuple-element.32) | copy-start | bytes 5505028
  62.8 3.0 %copy-start.2 = (bf16[896,512]{1,0:T(8,128)(2,1)}, bf16[896,512]{1,0:T(8,128)(2,1)S(1)}, u32[]{:S(2)}) copy-start(bf16[896,512]{1,0:T(8,128)(2,1)S(1)} %get-tuple-element.65.up_grad_ref) | copy-start | bytes 2752516
  62.8 3.0 %copy-start.1 = (bf16[1,896,2048]{2,1,0:T(8,128)(2,1)S(1)}, bf16[1,896,2048]{2,1,0:T(8,128)(2,1)}, u32[]{:S(2)}) copy-start(bf16[1,896,2048]{2,1,0:T(8,128)(2,1)} %param.25) | copy-start | bytes 11010052
  65.8 4.6 %copy-start.15 = (f32[128]{0:T(128)S(1)}, f32[128]{0:T(128)}, u32[]{:S(2)}) copy-start(f32[128]{0:T(128)} %param.20) | copy-start | bytes 1540
  65.8 5.3 %copy-start.14 = (f32[4,128]{1,0:T(4,128)S(1)}, f32[4,128]{1,0:T(4,128)}, u32[]{:S(2)}) copy-start(f32[4,128]{1,0:T(4,128)} %param.31) | copy-start | bytes 6148
  113.2 4.7 %copy-start.5 = (bf16[128,2048]{1,0:T(8,128)(2,1)S(1)}, bf16[128,2048]{1,0:T(8,128)(2,1)}, u32[]{:S(2)}) copy-start(bf16[128,2048]{1,0:T(8,128)(2,1)} %get-tuple-element.37) | copy-start | bytes 1572868
  114.6 4.5 %copy-start.10 = (bf16[128,256]{1,0:T(8,128)(2,1)S(1)}, bf16[128,256]{1,0:T(8,128)(2,1)}, u32[]{:S(2)}) copy-start(bf16[128,256]{1,0:T(8,128)(2,1)} %param.27) | copy-start | bytes 196612
  117.9 22.6 %copy-start.11 = (bf16[128,256]{1,0:T(8,128)(2,1)S(1)}, bf16[128,256]{1,0:T(8,128)(2,1)}, u32[]{:S(2)}) copy-start(bf16[128,256]{1,0:T(8,128)(2,1)} %param.28) | copy-start | bytes 196612
  118.4 23.8 %copy-start.12 = (bf16[128,256]{1,0:T(8,128)(2,1)S(1)}, bf16[128,256]{1,0:T(8,128)(2,1)}, u32[]{:S(2)}) copy-start(bf16[128,256]{1,0:T(8,128)(2,1)} %param.29) | copy-start | bytes 196612
  139.5 4.3 %copy-start.8 = (f32[1,4,64,64]{3,2,1,0:T(8,128)S(1)}, f32[1,4,64,64]{3,2,1,0:T(8,128)}, u32[]{:S(2)}) copy-start(f32[1,4,64,64]{3,2,1,0:T(8,128)} %param.32) | copy-start | bytes 196612
  141.2 3.9 %copy-start.6 = (bf16[8,128,256]{2,1,0:T(8,128)(2,1)S(1)}, bf16[8,128,256]{2,1,0:T(8,128)(2,1)}, u32[]{:S(2)}) copy-start(bf16[8,128,256]{2,1,0:T(8,128)(2,1)} %get-tuple-element.40) | copy-start | bytes 1572868
  141.2 3.9 %copy-start.7 = (bf16[8,128,256]{2,1,0:T(8,128)(2,1)S(1)}, bf16[8,128,256]{2,1,0:T(8,128)(2,1)}, u32[]{:S(2)}) copy-start(bf16[8,128,256]{2,1,0:T(8,128)(2,1)} %get-tuple-element.39) | copy-start | bytes 1572868
  146.2 4.5 %copy-start.3 = (bf16[896,2048]{1,0:T(8,128)(2,1)S(1)}, bf16[896,2048]{1,0:T(8,128)(2,1)}, u32[]{:S(2)}) copy-start(bf16[896,2048]{1,0:T(8,128)(2,1)} %get-tuple-element.36) | copy-start | bytes 11010052
  150.7 1.8 %copy-start.9 = (bf16[128,512]{1,0:T(8,128)(2,1)S(1)}, bf16[128,512]{1,0:T(8,128)(2,1)}, u32[]{:S(2)}) copy-start(bf16[128,512]{1,0:T(8,128)(2,1)} %get-tuple-element.84) | copy-start | bytes 393220
